TPU v7x, 32 devices: a whole 2x2x4 slice. The times are simulated.
32 devices in a mesh: fs: 4 (over z), rep: 4 (over y, x), tp: 2 (over core).
Axes of the slice: x: 2, y: 2, z: 4, core: 2. Of those that a mesh axis runs over, the one named last changes fastest.
Arguments:
- normed_in: bfloat16 [24576, 2048], P(('fs', 'rep')), may hold values from -6 to 6
- cotan_rec: bfloat16 [24576, 2048], P(('fs', 'rep'), 'tp'), may hold values from -0.0390625 to 0.0390625
- cotan_gate: bfloat16 [24576, 2048], P(('fs', 'rep'), 'tp'), may hold values from -0.0390625 to 0.0390625
- factor_rec: bfloat16 [2048, 512], P('fs'), may hold values from -0.125 to 0.125
- factor_gate: bfloat16 [2048, 512], P('fs'), may hold values from -0.125 to 0.125
- first_rec: float32 [512, 2048], P('fs', 'tp'), may hold values from -6 to 6
- first_gate: float32 [512, 2048], P('fs', 'tp'), may hold values from -6 to 6
- second_rec: float32 [512, 2048], P('fs', 'tp'), may hold values from 0.25 to 4
- second_gate: float32 [512, 2048], P('fs', 'tp'), may hold values from 0.25 to 4
- master_rec: float32 [2048, 2048], P('fs', 'tp'), may hold values from -0.125 to 0.125
- master_gate: float32 [2048, 2048], P('fs', 'tp'), may hold values from -0.125 to 0.125
Outputs:
- update_rec: float32 [2048, 2048], P('fs', 'tp')
- update_gate: float32 [2048, 2048], P('fs', 'tp')
- new_first_rec: float32 [512, 2048], P('fs', 'tp')
- new_first_gate: float32 [512, 2048], P('fs', 'tp')
- new_second_rec: float32 [512, 2048], P('fs', 'tp')
- new_second_gate: float32 [512, 2048], P('fs', 'tp')
- copy_rec: bfloat16 [2048, 2048], P(None, 'tp')
- copy_gate: bfloat16 [2048, 2048], P(None, 'tp')
All inputs are finite; a program needn't handle non-finite values.
Results may differ from a plain program's by a relative error of at most 0.007.
Values may be sent and summed in bfloat16 or wider, within the bound.
A program may use at most 128 MiB of HBM per device.

v0:
```python
import functools

import jax
import jax.numpy as jnp
from jax import lax
from jax.experimental import pallas as pl
from jax.experimental.pallas import tpu as pltpu
from jax.sharding import PartitionSpec as P

beta_first = 0.8
beta_second = 0.9
scale_floor = 0.25
step_rate = 0.01

MESH = pl.DeviceIdType.MESH
F32 = jnp.float32
BF16 = jnp.bfloat16
TOKEN_TILES = 4


def kernel(
    nf,
    nr,
    x_hbm,
    c0_hbm,
    c1_hbm,
    fac0_hbm,
    fac1_hbm,
    first0,
    first1,
    second0,
    second1,
    mast_hbm,
    fac_out,
    dir_out,
    low_out,
    mast_out,
    sum_out,
    x,
    c,
    fac,
    proj,
    part,
    own,
    recv_rep,
    mid,
    recv_fs,
    fst,
    snd,
    low,
    dirs,
    sums,
    sums_in,
    mast,
    local_sem,
    out_sem,
    fz_s,
    fz_r,
    fr_s,
    fr_r,
    fx_s,
    fx_r,
    pj_s,
    pj_r,
    rr_s,
    rr_r,
    rf_s,
    rf_r,
    dz_s,
    dz_r,
    dr_s,
    dr_r,
    lw_s,
    lw_r,
    sm_s,
    sm_r,
    mz_s,
    mz_r,
    mr_s,
    mr_r,
):
    f, r, t = lax.axis_index("fs"), lax.axis_index("rep"), lax.axis_index("tp")
    tokens = x.shape[0]
    rank, cols = dirs.shape[1], dirs.shape[2]
    rows = fac0_hbm.shape[0]
    quarter = rows // nr
    low_rows = rank // nf
    width = cols // nr
    tile = tokens // TOKEN_TILES

    def fpeer(k):
        return lax.rem(f + k, nf)

    def rpeer(k):
        return lax.rem(r + k, nr)

    mine = fac.at[t, pl.ds(pl.multiple_of(f * rows, rows), rows), :]

    @pl.when(t == 0)
    def _():
        pltpu.make_async_copy(fac0_hbm, mine, local_sem.at[0]).start()

    @pl.when(t != 0)
    def _():
        pltpu.make_async_copy(fac1_hbm, mine, local_sem.at[0]).start()

    load_m = pltpu.make_async_copy(
        mast_hbm, mast.at[pl.ds(pl.multiple_of(f * rows, rows), rows), :], local_sem.at[8]
    )
    load_m.start()
    load_x = pltpu.make_async_copy(x_hbm, x, local_sem.at[1])
    load_x.start()
    loads = [
        pltpu.make_async_copy(c0_hbm, c.at[0], local_sem.at[2]),
        pltpu.make_async_copy(c1_hbm, c.at[1], local_sem.at[3]),
    ]
    lane = pl.ds(pl.multiple_of(r * width, width), width)
    for i, (src, dst) in enumerate(
        ((first0, fst.at[0]), (first1, fst.at[1]), (second0, snd.at[0]), (second1, snd.at[1]))
    ):
        loads.append(pltpu.make_async_copy(src.at[:, lane], dst, local_sem.at[4 + i]))
    for load in loads:
        load.start()

    barrier = pltpu.get_barrier_semaphore()
    for k in range(1, nf):
        pl.semaphore_signal(barrier, inc=1, device_id=(fpeer(k), r, t), device_id_type=MESH)
    for k in range(1, nr):
        pl.semaphore_signal(barrier, inc=1, device_id=(f, rpeer(k), t), device_id_type=MESH)
    pl.semaphore_signal(barrier, inc=1, device_id=(f, r, 1 - t), device_id_type=MESH)
    pl.semaphore_wait(barrier, nf + nr - 1)

    started = []

    def send(src, dst, s_sem, r_sem, device):
        copy = pltpu.make_async_remote_copy(
            src_ref=src, dst_ref=dst, send_sem=s_sem, recv_sem=r_sem,
            device_id=device, device_id_type=MESH,
        )
        copy.start()
        started.append(copy)

    def arrived(ref, s_sem, r_sem, device):
        pltpu.make_async_remote_copy(
            src_ref=ref, dst_ref=ref, send_sem=s_sem, recv_sem=r_sem,
            device_id=device, device_id_type=MESH,
        ).wait_recv()

    sibling = (f, r, 1 - t)

    def fpiece(ff, rr):
        start = pl.multiple_of(ff * rows + rr * quarter, quarter)
        return fac.at[t, pl.ds(start, quarter), :]

    pltpu.make_async_copy(fac0_hbm, mine, local_sem.at[0]).wait()
    for k in range(1, nf):
        send(fpiece(f, r), fpiece(f, r), fz_s.at[k - 1], fz_r.at[k - 1], (fpeer(k), r, t))

    def mpiece(ff, rr):
        start = pl.multiple_of(ff * rows + rr * quarter, quarter)
        return mast.at[pl.ds(start, quarter), :]

    def pass_master(k):
        src = fpeer(nf - k)
        arrived(mpiece(src, r), mz_s.at[k - 1], mz_r.at[k - 1], (src, r, t))
        for j in range(1, nr):
            send(mpiece(src, r), mpiece(src, r), mr_s.at[k - 1, j - 1], mr_r.at[k - 1, j - 1], (f, rpeer(j), t))

    third = (nf - 1) // 3
    load_m.wait()
    for k in range(1, nf):
        send(mpiece(f, r), mpiece(f, r), mz_s.at[k - 1], mz_r.at[k - 1], (fpeer(k), r, t))
    for k in range(1, nf):
        src = fpeer(nf - k)
        arrived(fpiece(src, r), fz_s.at[k - 1], fz_r.at[k - 1], (src, r, t))
        for j in range(1, nr):
            send(fpiece(src, r), fpiece(src, r), fr_s.at[k - 1, j - 1], fr_r.at[k - 1, j - 1], (f, rpeer(j), t))
    for k in range(1, nf):
        src = fpeer(nf - k)
        for j in range(1, nr):
            rsrc = rpeer(nr - j)
            arrived(fpiece(src, rsrc), fr_s.at[k - 1, j - 1], fr_r.at[k - 1, j - 1], (f, rsrc, t))

    for k in range(1, 1 + third):
        pass_master(k)

    load_x.wait()
    for i in range(TOKEN_TILES):
        span = pl.ds(i * tile, tile)
        proj[t, span, :] = jnp.dot(
            x[span, :], fac[t], preferred_element_type=F32
        ).astype(BF16)
        send(proj.at[t, span, :], proj.at[t, span, :], pj_s.at[i], pj_r.at[i], sibling)
    send(fac.at[t], fac.at[t], fx_s, fx_r, sibling)
    for load in loads:
        load.wait()

    def product(p, rr):
        at = pl.ds(pl.multiple_of(rr * width, width), width)
        return lax.dot_general(
            proj[p], c[p, :, at], (((0,), (0,)), ((), ())), preferred_element_type=F32
        )

    order = (t, 1 - t)
    for s, p in enumerate(order):
        if s == 1:
            for i in range(TOKEN_TILES):
                span = pl.ds(i * tile, tile)
                arrived(proj.at[1 - t, span, :], pj_s.at[i], pj_r.at[i], sibling)
        for j in range(1, nr):
            part[s, j - 1] = product(p, rpeer(j)).astype(BF16)
            send(part.at[s, j - 1], recv_rep.at[s, j - 1], rr_s.at[s, j - 1], rr_r.at[s, j - 1], (f, rpeer(j), t))
        own[s] = product(p, r)

    for k in range(1 + third, 1 + 2 * third):
        pass_master(k)

    def rank_rows(ff):
        return pl.ds(pl.multiple_of(ff * low_rows, low_rows), low_rows)

    for s in range(2):
        for j in range(1, nr):
            arrived(recv_rep.at[s, j - 1], rr_s.at[s, j - 1], rr_r.at[s, j - 1], (f, rpeer(nr - j), t))
        total = own[s]
        for j in range(1, nr):
            total = total + recv_rep[s, j - 1].astype(F32)
        own[s] = total
        mid[s] = total.astype(BF16)
        for k in range(1, nf):
            send(mid.at[s, rank_rows(fpeer(k)), :], recv_fs.at[s, k - 1], rf_s.at[s, k - 1], rf_r.at[s, k - 1], (fpeer(k), r, t))

    def dpiece(p, ff, rr):
        at = pl.ds(pl.multiple_of(rr * width, width), width)
        return dirs.at[p, rank_rows(ff), at]

    for s, p in enumerate(order):
        for k in range(1, nf):
            arrived(recv_fs.at[s, k - 1], rf_s.at[s, k - 1], rf_r.at[s, k - 1], (fpeer(nf - k), r, t))
        total = own[s, rank_rows(f), :]
        for k in range(1, nf):
            total = total + recv_fs[s, k - 1].astype(F32)
        rounded = total.astype(BF16)
        low[p, :, lane] = rounded
        wide = rounded.astype(F32)
        new_first = beta_first * fst[p] + (1.0 - beta_first) * wide
        new_second = beta_second * snd[p] + (1.0 - beta_second) * wide * wide
        dirs[p, rank_rows(f), lane] = (new_first / jnp.sqrt(new_second)).astype(BF16)
        for k in range(1, nf):
            send(dpiece(p, f, r), dpiece(p, f, r), dz_s.at[s, k - 1], dz_r.at[s, k - 1], (fpeer(k), r, t))
        for j in range(1, nr):
            send(dpiece(p, f, r), dpiece(p, f, r), dr_s.at[s, 0, j - 1], dr_r.at[s, 0, j - 1], (f, rpeer(j), t))
    for k in range(1 + 2 * third, nf):
        pass_master(k)
    for s, p in enumerate(order):
        for k in range(1, nf):
            src = fpeer(nf - k)
            arrived(dpiece(p, src, r), dz_s.at[s, k - 1], dz_r.at[s, k - 1], (src, r, t))
            for j in range(1, nr):
                send(dpiece(p, src, r), dpiece(p, src, r), dr_s.at[s, k, j - 1], dr_r.at[s, k, j - 1], (f, rpeer(j), t))
    for j in range(1, nr):
        send(low.at[:, :, lane], low.at[:, :, lane], lw_s.at[j - 1], lw_r.at[j - 1], (f, rpeer(j), t))

    outs = []

    def put(src, dst):
        copy = pltpu.make_async_copy(src, dst, out_sem.at[len(outs)])
        copy.start()
        outs.append(copy)

    arrived(fac.at[1 - t], fx_s, fx_r, sibling)
    put(fac, fac_out)
    for s, p in enumerate(order):
        for k in range(nf):
            src = fpeer(nf - k)
            for j in range(1, nr):
                rsrc = rpeer(nr - j)
                arrived(dpiece(p, src, rsrc), dr_s.at[s, k, j - 1], dr_r.at[s, k, j - 1], (f, rsrc, t))
    put(dirs, dir_out)

    for p in range(2):
        square = dirs[p].astype(F32)
        square = square * square
        sums[p] = jnp.sum(square.reshape(rank // 8, 8, cols), axis=0)
    send(sums, sums_in, sm_s, sm_r, sibling)
    for j in range(1, nr):
        rsrc = rpeer(nr - j)
        at = pl.ds(pl.multiple_of(rsrc * width, width), width)
        arrived(low.at[:, :, at], lw_s.at[j - 1], lw_r.at[j - 1], (f, rsrc, t))
    put(low, low_out)
    for k in range(1, nf):
        src = fpeer(nf - k)
        for j in range(1, nr):
            rsrc = rpeer(nr - j)
            arrived(mpiece(src, rsrc), mr_s.at[k - 1, j - 1], mr_r.at[k - 1, j - 1], (f, rsrc, t))
    put(mast, mast_out)
    arrived(sums_in, sm_s, sm_r, sibling)
    for p in range(2):
        sum_out[p] = sums[p] + sums_in[p]
    for copy in outs:
        copy.wait()
    for copy in started:
        copy.wait_send()


def gather_directions(nf, nr, normed_in, cotans, factors, firsts, seconds, master):
    tokens, model = normed_in.shape
    cols = cotans[0].shape[1]
    rows, rank = factors[0].shape
    low_rows, width = rank // nf, cols // nr
    dma = pltpu.SemaphoreType.DMA
    anyspec = pl.BlockSpec(memory_space=pl.ANY)
    pair = lambda *shape: [dma(shape), dma(shape)]
    return pl.pallas_call(
        functools.partial(kernel, nf, nr),
        out_shape=(
            jax.ShapeDtypeStruct((2, model, rank), BF16),
            jax.ShapeDtypeStruct((2, rank, cols), BF16),
            jax.ShapeDtypeStruct((2, low_rows, cols), BF16),
            jax.ShapeDtypeStruct((model, master.shape[1]), BF16),
            jax.ShapeDtypeStruct((2, 8, cols), F32),
        ),
        in_specs=[anyspec] * 10,
        out_specs=(anyspec, anyspec, anyspec, anyspec, pl.BlockSpec(memory_space=pltpu.VMEM)),
        scratch_shapes=[
            pltpu.VMEM((tokens, model), BF16),
            pltpu.VMEM((2, tokens, cols), BF16),
            pltpu.VMEM((2, model, rank), BF16),
            pltpu.VMEM((2, tokens, rank), BF16),
            pltpu.VMEM((2, nr - 1, rank, width), BF16),
            pltpu.VMEM((2, rank, width), F32),
            pltpu.VMEM((2, nr - 1, rank, width), BF16),
            pltpu.VMEM((2, rank, width), BF16),
            pltpu.VMEM((2, nf - 1, low_rows, width), BF16),
            pltpu.VMEM((2, low_rows, width), F32),
            pltpu.VMEM((2, low_rows, width), F32),
            pltpu.VMEM((2, low_rows, cols), BF16),
            pltpu.VMEM((2, rank, cols), BF16),
            pltpu.VMEM((2, 8, cols), F32),
            pltpu.VMEM((2, 8, cols), F32),
            pltpu.VMEM((model, master.shape[1]), BF16),
            dma((9,)),
            dma((4,)),
            *pair(nf - 1),
            *pair(nf - 1, nr - 1),
            dma,
            dma,
            *pair(TOKEN_TILES),
            *pair(2, nr - 1),
            *pair(2, nf - 1),
            *pair(2, nf - 1),
            *pair(2, nf, nr - 1),
            *pair(nr - 1),
            dma,
            dma,
            *pair(nf - 1),
            *pair(nf - 1, nr - 1),
        ],
        cost_estimate=pl.CostEstimate(
            flops=10 * tokens * model * rank, bytes_accessed=400 * 2**20, transcendentals=0
        ),
        compiler_params=pltpu.CompilerParams(
            collective_id=0, has_side_effects=True, vmem_limit_bytes=60 * 2**20
        ),
    )(normed_in, *cotans, *factors, *firsts, *seconds, master)


def body(
    nf,
    nr,
    nt,
    normed_in,
    cotan_rec,
    cotan_gate,
    factor_rec,
    factor_gate,
    first_rec,
    first_gate,
    second_rec,
    second_gate,
    master_rec,
    master_gate,
):
    r = lax.axis_index("rep")
    factors = (factor_rec, factor_gate)
    firsts = (first_rec, first_gate)
    seconds = (second_rec, second_gate)
    piece = master_rec.shape[0] // nr
    half = 3 * master_gate.shape[1] // 4

    def gathered(m):
        own = lax.dynamic_slice_in_dim(m, r * piece, piece, 0).astype(BF16)
        return lax.all_gather(own, ("fs", "rep"), axis=0, tiled=True)

    whole_rec = gathered(master_rec)
    gate_right = gathered(master_gate[:, half:])
    fac, dirs, low, gate_left, sums = gather_directions(
        nf, nr, normed_in, (cotan_rec, cotan_gate), factors, firsts, seconds,
        master_gate[:, :half].astype(BF16),
    )
    wholes = (whole_rec, jnp.concatenate((gate_left, gate_right), axis=1))
    entries = float(dirs.shape[1] * dirs.shape[2] * nt)
    updates, new_firsts, new_seconds, copies = [], [], [], []
    for p in range(2):
        scale = 1.0 / jnp.sqrt(jnp.sum(sums[p]) / entries + scale_floor)
        updates.append(jnp.dot(factors[p], dirs[p], preferred_element_type=F32) * scale)
        wide = low[p].astype(F32)
        new_firsts.append(beta_first * firsts[p] + (1.0 - beta_first) * wide)
        new_seconds.append(beta_second * seconds[p] + (1.0 - beta_second) * wide * wide)
        upd = jnp.dot(fac[p], dirs[p], preferred_element_type=F32) * scale
        copies.append((wholes[p].astype(F32) - step_rate * upd).astype(BF16))
    return (*updates, *new_firsts, *new_seconds, *copies)


def solution(mesh):
    nf, nr, nt = mesh.shape["fs"], mesh.shape["rep"], mesh.shape["tp"]
    return jax.shard_map(
        functools.partial(body, nf, nr, nt),
        mesh=mesh,
        in_specs=(
            P(("fs", "rep"), None),
            P(("fs", "rep"), "tp"),
            P(("fs", "rep"), "tp"),
            P("fs", None),
            P("fs", None),
            P("fs", "tp"),
            P("fs", "tp"),
            P("fs", "tp"),
            P("fs", "tp"),
            P("fs", "tp"),
            P("fs", "tp"),
        ),
        out_specs=(
            P("fs", "tp"),
            P("fs", "tp"),
            P("fs", "tp"),
            P("fs", "tp"),
            P("fs", "tp"),
            P("fs", "tp"),
            P(None, "tp"),
            P(None, "tp"),
        ),
        check_vma=False,
    )
```

profile of v0, /device:TPU:0, one launch (start us, length us, event | category | flops | bytes accessed | tf_op | source)
XLA Modules:
  0.0 187.9 jit_solution(4987716220655002658)
XLA Ops:
  7.2 0.0 copy-start
  7.2 0.0 all-gather.5.cloned.1.call-start
  7.2 1.2 slice.41
  8.4 0.6 dynamic-slice_convert_fusion.1
  9.1 0.0 all-gather.5.cloned.1.call-update
  9.1 0.0 all-gather.3.cloned.1.call-start
  9.2 0.0 copy-done
  9.2 0.7 dynamic-slice_convert_fusion
  9.9 0.0 all-gather.3.cloned.1.call-update
  9.9 2.4 %slice.75.mast_hbm = bf16[512,768]{1,0:T(8,128)(2,1)} slice(f32[512,1024]{1,0:T(8,128)} %param.21), slice={[0:512], [0:768]} | slice | bytes 1572864 | tf_op jit(solution)/shard_map/slice | solution.py:398
  12.3 0.0 copy-start.3
  12.3 124.1 %shard_map.170 = (bf16[2,2048,512]{2,1,0:T(8,128)(2,1)}, bf16[2,512,1024]{2,1,0:T(8,128)(2,1)}, bf16[2,128,1024]{2,1,0:T(8,128)(2,1)}, bf16[2048,768]{1,0:T(8,128)(2,1)}, f32[2,8,1024]{2,1,0:T(8,128)}) custom-call(bf16[1536,2048]{1,0:T(8,128)(2,1)} %x_hbm.1, bf16[1536,1024]{1,0:T(8,128)(2,1)} %c0_hbm.1, bf16[1536,1024]{1,0:T(8,128)(2,1)} %c1_hbm.1, ...), custom_call_target="tpu_custom_call" | custom-call | flops 16106127360 | bytes 419430400 | tf_op jit(solution)/shard_map/pallas_call | solution.py:313
  136.4 1.4 slice_reduce_fusion
  139.2 0.0 copy-done.3
  139.2 3.3 %multiply_bitcast_fusion = f32[512,1024]{0,1:T(8,128)} fusion(bf16[512,512]{1,0:T(8,128)(2,1)S(1)} %copy-done.3, f32[]{:T(128)S(6)} %sqrt.7, bf16[2,512,1024]{2,1,0:T(8,128)(2,1)} %get-tuple-element.13), kind=kOutput, calls=%fused_computation.6 | convolution fusion | flops 537395200 | bytes 3670020 | tf_op jit(solution)/shard_map/dot_general | solution.py:405
  142.5 2.9 %copy.20 = f32[512,1024]{1,0:T(8,128)} copy(f32[512,1024]{0,1:T(8,128)} %multiply_bitcast_fusion) | data formatting | bytes 4194304
  145.4 0.0 copy-start.1
  145.4 0.0 copy-start.2
  145.4 3.5 %multiply_bitcast_fusion.1 = f32[512,1024]{0,1:T(8,128)} fusion(bf16[512,512]{1,0:T(8,128)(2,1)} %fac0_hbm.1, f32[]{:T(128)S(6)} %sqrt.6, bf16[2,512,1024]{2,1,0:T(8,128)(2,1)} %get-tuple-element.13), kind=kOutput, calls=%fused_computation.7 | convolution fusion | flops 537395200 | bytes 3670020 | tf_op jit(solution)/shard_map/dot_general | solution.py:405
  148.9 2.9 %copy.19 = f32[512,1024]{1,0:T(8,128)} copy(f32[512,1024]{0,1:T(8,128)} %multiply_bitcast_fusion.1) | data formatting | bytes 4194304
  151.8 0.0 copy-done.1
  151.8 0.0 copy-done.2
  151.8 2.9 %fusion.15 = (f32[128,1024]{1,0:T(8,128)}, f32[128,1024]{1,0:T(8,128)}, f32[128,1024]{1,0:T(8,128)}, f32[128,1024]{1,0:T(8,128)}) fusion(f32[128,1024]{1,0:T(8,128)} %second1.1, bf16[2,128,1024]{2,1,0:T(8,128)(2,1)} %get-tuple-element.15, f32[128,1024]{1,0:T(8,128)} %second0.1, f32[128,1024]{1,0:T(8,128)S(1)} %copy-done.2, f32[128,1024]{1,0:T(8,128)S(1)} %copy-done.1), kind=kLoop, calls=%fused_computation.26 | loop fusion | flops 2097152 | bytes 4718592 | tf_op jit(solution)/shard_map/add | solution.py:408
  154.6 0.0 all-gather.5.cloned.1.call-done
  154.6 7.8 %subtract_convert_fusion = bf16[2048,1024]{1,0:T(8,128)(2,1)} fusion(bf16[2048,256]{1,0:T(8,128)(2,1)} %all-gather.5.cloned.1.call-done, bf16[2048,768]{1,0:T(8,128)(2,1)} %get-tuple-element.17, f32[]{:T(128)S(6)} %sqrt.7, bf16[2,2048,512]{2,1,0:T(8,128)(2,1)} %get-tuple-element.16, bf16[2,512,1024]{2,1,0:T(8,128)(2,1)} %get-tuple-element.13), kind=kOutput, calls=%fused_computation | convolution fusion | flops 2164260864 | bytes 11534340 | tf_op jit(solution)/shard_map/dot_general | solution.py:409
  162.5 10.8 %all-gather.3.cloned.1.call-done = bf16[2048,1024]{1,0:T(8,128)(2,1)} async-done(((bf16[128,1024]{1,0:T(8,128)(2,1)}), bf16[2048,1024]{1,0:T(8,128)(2,1)}) %all-gather.3.cloned.1.call-update) | async-done | bytes 4194320 | tf_op jit(solution)/shard_map/all_gather | solution.py:392
  173.3 7.8 %subtract_convert_fusion.1 = bf16[2048,1024]{1,0:T(8,128)(2,1)} fusion(bf16[2048,1024]{1,0:T(8,128)(2,1)} %all-gather.3.cloned.1.call-done, f32[]{:T(128)S(6)} %sqrt.6, bf16[2,2048,512]{2,1,0:T(8,128)(2,1)} %get-tuple-element.16, bf16[2,512,1024]{2,1,0:T(8,128)(2,1)} %get-tuple-element.13), kind=kOutput, calls=%fused_computation.1 | convolution fusion | flops 2157969408 | bytes 11534340 | tf_op jit(solution)/shard_map/dot_general | solution.py:409
Async XLA Ops:
  7.2 2.0 %copy-start = (f32[512,1024]{1,0:T(8,128)S(1)}, f32[512,1024]{1,0:T(8,128)}, u32[]{:S(2)}) copy-start(f32[512,1024]{1,0:T(8,128)} %param.20) | copy-start | bytes 6291460
  7.2 147.5 %all-gather.5.cloned.1.call-start = ((), (), s32[]{:S(2)}) async-start(), calls=%async_computation.1 | async-start | bytes 1114112 | tf_op jit(solution)/shard_map/all_gather | solution.py:392
  9.1 164.2 %all-gather.3.cloned.1.call-start = ((), (), s32[]{:S(2)}) async-start(), calls=%async_computation | async-start | bytes 4456448 | tf_op jit(solution)/shard_map/all_gather | solution.py:392
  12.3 126.9 %copy-start.3 = (bf16[512,512]{1,0:T(8,128)(2,1)S(1)}, bf16[512,512]{1,0:T(8,128)(2,1)}, u32[]{:S(2)}) copy-start(bf16[512,512]{1,0:T(8,128)(2,1)} %fac1_hbm.1) | copy-start | bytes 1572868
  145.4 6.4 %copy-start.1 = (f32[128,1024]{1,0:T(8,128)S(1)}, f32[128,1024]{1,0:T(8,128)}, u32[]{:S(2)}) copy-start(f32[128,1024]{1,0:T(8,128)} %first0.1) | copy-start | bytes 1572868
  145.4 6.4 %copy-start.2 = (f32[128,1024]{1,0:T(8,128)S(1)}, f32[128,1024]{1,0:T(8,128)}, u32[]{:S(2)}) copy-start(f32[128,1024]{1,0:T(8,128)} %first1.1) | copy-start | bytes 1572868
Sparse Core Ops, SparseCore 0:
  10.7 74.7 all-gather.4
  88.8 84.3 all-gather.2
where the time goes:
time: 188 us
  Pallas kernels  124 us (66%)
  matrix products  22.4 us (12%)
  between operations  15.5 us (8%)
  waiting for transfers between devices  10.8 us (6%)
  local copies, waits for them, and re-layouts  10.7 us (6%)
  other arithmetic  4.26 us (2%)
    pallas_call x1, Pallas kernels, gather_directions(): pl.pallas_call(functools.partial(kernel, nf, nr), out_shape=(jax.ShapeDty...  124 us
    dot_general x2, matrix products, body(): upd = jnp.dot(fac[p], dirs[p], preferred_element_type=F32) * scale  15.6 us
    all_gather x2, waiting for transfers between devices, gathered(): return lax.all_gather(own, ('fs', 'rep'), axis=0, tiled=True)  10.8 us
    dot_general x2, matrix products, body(): jnp.dot(factors[p], dirs[p], preferred_element_type=F32) * scale  6.83 us
    unnamed x10, local copies, waits for them, and re-layouts  5.78 us
  transfers between devices with their start and end apart: 2, of which 1 were waited for; matrix products, arithmetic and copies ran while one was open for 15% of the time, Pallas kernels for 66%

commit v1 on v0

v1 whole, which is shorter than its diff:
```python
import functools

import jax
import jax.numpy as jnp
from jax import lax
from jax.experimental import pallas as pl
from jax.experimental.pallas import tpu as pltpu
from jax.sharding import PartitionSpec as P

beta_first = 0.8
beta_second = 0.9
scale_floor = 0.25
step_rate = 0.01

MESH = pl.DeviceIdType.MESH
F32 = jnp.float32
BF16 = jnp.bfloat16
TOKEN_TILES = 4
HALF_CHUNKS = 2
CHUNKS = 2 * HALF_CHUNKS
SHARES = {
    "factors": 0.0,
    "projection": 0.0,
    "products": 0.17,
    "stage": 0.34,
    "reduce": 0.42,
    "directions": 0.5,
    "gather": 1.0,
}


def kernel(
    nf,
    nr,
    x_hbm,
    c0_hbm,
    c1_hbm,
    fac0_hbm,
    fac1_hbm,
    first0,
    first1,
    second0,
    second1,
    mast0_hbm,
    mast1_hbm,
    fac_out,
    dir_out,
    low_out,
    mast_out,
    sum_out,
    x,
    c,
    fac,
    acc,
    proj,
    part,
    recv,
    keep,
    own,
    mid,
    recv_fs,
    fst,
    snd,
    low,
    dirs,
    wide,
    mast,
    sums,
    sums_z,
    sums_r,
    sums_t,
    local_sem,
    out_sem,
    oz_sem,
    op_sem,
    fz_s,
    fz_r,
    fp_s,
    fp_r,
    fd_s,
    fd_r,
    fx_s,
    fx_r,
    pj_s,
    pj_r,
    rp_s,
    rp_r,
    rf_s,
    rf_r,
    dz_s,
    dz_r,
    dp_s,
    dp_r,
    dd_s,
    dd_r,
    lw_s,
    lw_r,
    sz_s,
    sz_r,
    sr_s,
    sr_r,
    st_s,
    st_r,
    mz_s,
    mz_r,
    mp_s,
    mp_r,
):
    f, r, t = lax.axis_index("fs"), lax.axis_index("rep"), lax.axis_index("tp")
    tokens = x.shape[0]
    rank, cols = dirs.shape[1], dirs.shape[2]
    rows = fac0_hbm.shape[0]
    half, quarter = rows // 2, rows // nr
    low_rows = rank // nf
    low_half = low_rows // 2
    width = cols // nr
    tile = tokens // TOKEN_TILES
    side = nr // 2
    rx, ry = lax.rem(r, side), r // side
    across = (ry * side + 1 - rx, (1 - ry) * side + rx)
    corner = (1 - ry) * side + 1 - rx
    sibling = (f, r, 1 - t)

    def fpeer(k):
        return lax.rem(f + k, nf)

    def rpeer(k):
        return lax.rem(r + k, nr)

    def block(ff):
        return pl.ds(pl.multiple_of(ff * rows, rows), rows)

    mine = fac.at[t, block(f), :]

    @pl.when(t == 0)
    def _():
        pltpu.make_async_copy(fac0_hbm, mine, local_sem.at[0]).start()

    @pl.when(t != 0)
    def _():
        pltpu.make_async_copy(fac1_hbm, mine, local_sem.at[0]).start()

    load_m = [
        pltpu.make_async_copy(mast0_hbm, wide.at[0], local_sem.at[8]),
        pltpu.make_async_copy(mast1_hbm, wide.at[1], local_sem.at[9]),
    ]
    load_x = pltpu.make_async_copy(x_hbm, x, local_sem.at[1])
    for load in (*load_m, load_x):
        load.start()
    load_c = [
        pltpu.make_async_copy(c0_hbm, c.at[0], local_sem.at[2]),
        pltpu.make_async_copy(c1_hbm, c.at[1], local_sem.at[3]),
    ]
    lane = pl.ds(pl.multiple_of(r * width, width), width)
    load_s = []
    for i, (src, dst) in enumerate(
        ((first0, fst.at[0]), (first1, fst.at[1]), (second0, snd.at[0]), (second1, snd.at[1]))
    ):
        load_s.append(pltpu.make_async_copy(src.at[:, lane], dst, local_sem.at[4 + i]))
    for load in (*load_c, *load_s):
        load.start()

    barrier = pltpu.get_barrier_semaphore()
    for k in range(1, nf):
        pl.semaphore_signal(barrier, inc=1, device_id=(fpeer(k), r, t), device_id_type=MESH)
    for k in range(1, nr):
        pl.semaphore_signal(barrier, inc=1, device_id=(f, rpeer(k), t), device_id_type=MESH)
    pl.semaphore_signal(barrier, inc=1, device_id=sibling, device_id_type=MESH)
    pl.semaphore_wait(barrier, nf + nr - 1)

    started = []

    def remote(src, dst, s_sem, r_sem, device):
        return pltpu.make_async_remote_copy(
            src_ref=src, dst_ref=dst, send_sem=s_sem, recv_sem=r_sem,
            device_id=device, device_id_type=MESH,
        )

    def guarded(action, when):
        if when is None:
            action()
        else:
            pl.when(when)(lambda: action())

    def send(ref, s_sem, r_sem, device, dst=None, when=None):
        copy = remote(ref, ref if dst is None else dst, s_sem, r_sem, device)
        guarded(copy.start, when)
        started.append((copy, when))

    def arrived(ref, s_sem, r_sem, when=None):
        guarded(remote(ref, ref, s_sem, r_sem, sibling).wait_recv, when)

    outs = []

    def put(src, dst, sem, when=None):
        copy = pltpu.make_async_copy(src, dst, sem)
        guarded(copy.start, when)
        outs.append((copy, when))

    def fpiece(ff, rr, start=0, count=quarter):
        at = pl.multiple_of(ff * rows + rr * quarter + start, count)
        return fac.at[t, pl.ds(at, count), :]

    pltpu.make_async_copy(fac0_hbm, mine, local_sem.at[0]).wait()
    for k in range(1, nf):
        send(fpiece(f, r), fz_s.at[k - 1], fz_r.at[k - 1], (fpeer(k), r, t))

    chunk = half // HALF_CHUNKS
    line = (
        (lambda j: lax.rem(f + nf - j, nf), lambda j: f >= j, fpeer(1), f < nf - 1),
        (lambda j: lax.rem(f + j, nf), lambda j: f < nf - j, fpeer(nf - 1), f > 0),
    )

    def mpiece(ref, ff, ch, other=False):
        p = ch % 2
        h = rx if p == 0 else ry
        if other:
            h = 1 - h
        at = pl.multiple_of(ff * rows + h * half + (ch // 2) * chunk, chunk)
        return ref.at[p, pl.ds(at, chunk), :]

    for p in range(2):
        load_m[p].wait()
        mast[p, block(f), :] = wide[p].astype(BF16)
    for ch in range(CHUNKS):
        for d, (_, _, onto, there) in enumerate(line):
            send(mpiece(mast, f, ch), mz_s.at[d, 0, ch], mz_r.at[d, 0, ch], (onto, r, t), when=there)
    for p in range(2):
        put(mast.at[p, block(f), :], mast_out.at[p, block(f), :], out_sem.at[p])

    relays = [(j, ch) for j in range(1, nf) for ch in range(CHUNKS)]
    done = [0]

    def relay(point):
        upto = round(SHARES[point] * len(relays))
        for j, ch in relays[done[0]:upto]:
            for d, (source, exists, onto, there) in enumerate(line):
                piece = mpiece(mast, source(j), ch)
                arrived(piece, mz_s.at[d, j - 1, ch], mz_r.at[d, j - 1, ch], when=exists(j))
                if j < nf - 1:
                    send(piece, mz_s.at[d, j, ch], mz_r.at[d, j, ch], (onto, r, t), when=exists(j) & there)
                send(piece, mp_s.at[d, j - 1, ch], mp_r.at[d, j - 1, ch], (f, across[ch % 2], t), when=exists(j))
                put(piece, mpiece(mast_out, source(j), ch), oz_sem.at[d, j - 1, ch], when=exists(j))
        done[0] = max(done[0], upto)

    def project(ff, first=False):
        at = block(ff)
        for i in range(TOKEN_TILES):
            span = pl.ds(i * tile, tile)
            product = jnp.dot(x[span, at], fac[t, at, :], preferred_element_type=F32)
            acc[span, :] = product if first else acc[span, :] + product

    load_x.wait()
    project(f, first=True)

    for k in range(1, nf):
        src = fpeer(nf - k)
        arrived(fpiece(src, r), fz_s.at[k - 1], fz_r.at[k - 1])
        for a in range(2):
            send(fpiece(src, r), fp_s.at[a, k - 1], fp_r.at[a, k - 1], (f, across[a], t))
    fhalf = quarter // 2
    for k in range(1, nf):
        src = fpeer(nf - k)
        for a in range(2):
            arrived(fpiece(src, across[a]), fp_s.at[a, k - 1], fp_r.at[a, k - 1])
            send(
                fpiece(src, across[a], a * fhalf, fhalf), fd_s.at[a, k - 1], fd_r.at[a, k - 1],
                (f, across[1 - a], t),
            )
    relay("factors")
    for k in range(1, nf):
        src = fpeer(nf - k)
        for a in range(2):
            arrived(fpiece(src, corner, a * fhalf, fhalf), fd_s.at[a, k - 1], fd_r.at[a, k - 1])
        if k < nf - 1:
            project(src)
    at = block(fpeer(1))
    for i in range(TOKEN_TILES):
        span = pl.ds(i * tile, tile)
        product = jnp.dot(x[span, at], fac[t, at, :], preferred_element_type=F32)
        proj[t, :, span] = jnp.transpose(acc[span, :] + product).astype(BF16)
        send(proj.at[t, :, span], pj_s.at[i], pj_r.at[i], sibling)
    send(fac.at[t], fx_s, fx_r, sibling)
    relay("projection")
    for load in (*load_c, *load_s):
        load.wait()

    upper = rank // 2
    spans = (slice(0, upper), slice(upper, rank))

    def product(p, rr):
        at = pl.ds(pl.multiple_of(rr * width, width), width)
        return jnp.dot(proj[p], c[p, :, at], preferred_element_type=F32)

    def pass_part(s, m, a):
        send(part.at[s, m], rp_s.at[s, m], rp_r.at[s, m], (f, across[a], t), dst=recv.at[s, m])

    def got_part(s, m):
        arrived(recv.at[s, m], rp_s.at[s, m], rp_r.at[s, m])

    order = (t, 1 - t)
    for s, p in enumerate(order):
        if s == 1:
            for i in range(TOKEN_TILES):
                span = pl.ds(i * tile, tile)
                arrived(proj.at[1 - t, :, span], pj_s.at[i], pj_r.at[i])
        far = product(p, corner)
        for a in range(2):
            part[s, a] = far[spans[a]].astype(BF16)
            pass_part(s, a, a)
        for a in range(2):
            near = product(p, across[a])
            part[s, 2 + a] = near[spans[a]].astype(BF16)
            pass_part(s, 2 + a, a)
            keep[s, 1 - a] = near[spans[1 - a]]
        own[s] = product(p, r)
    relay("products")

    def rank_rows(ff):
        return pl.ds(pl.multiple_of(ff * low_rows, low_rows), low_rows)

    for s in range(2):
        for a in range(2):
            got_part(s, a)
            part[s, 4 + a] = (keep[s, a] + recv[s, a].astype(F32)).astype(BF16)
            pass_part(s, 4 + a, 1 - a)
    relay("stage")
    for s in range(2):
        for a in range(2):
            got_part(s, 2 + a)
            got_part(s, 4 + a)
            total = own[s, spans[a], :] + recv[s, 2 + a].astype(F32) + recv[s, 4 + a].astype(F32)
            own[s, spans[a], :] = total
            mid[s, spans[a], :] = total.astype(BF16)
        for k in range(1, nf):
            send(
                mid.at[s, rank_rows(fpeer(k)), :], rf_s.at[s, k - 1], rf_r.at[s, k - 1], (fpeer(k), r, t),
                dst=recv_fs.at[s, k - 1],
            )
    relay("reduce")

    def dpiece(p, ff, rr, start=0, count=low_rows):
        at = pl.ds(pl.multiple_of(rr * width, width), width)
        ranks = pl.ds(pl.multiple_of(ff * low_rows + start, count), count)
        return dirs.at[p, ranks, at]

    for s, p in enumerate(order):
        for k in range(1, nf):
            arrived(recv_fs.at[s, k - 1], rf_s.at[s, k - 1], rf_r.at[s, k - 1])
        total = own[s, rank_rows(f), :]
        for k in range(1, nf):
            total = total + recv_fs[s, k - 1].astype(F32)
        rounded = total.astype(BF16)
        low[p, :, lane] = rounded
        again = rounded.astype(F32)
        new_first = beta_first * fst[p] + (1.0 - beta_first) * again
        new_second = beta_second * snd[p] + (1.0 - beta_second) * again * again
        direction = (new_first / jnp.sqrt(new_second)).astype(BF16)
        dirs[p, rank_rows(f), lane] = direction
        for k in range(1, nf):
            send(dpiece(p, f, r), dz_s.at[s, k - 1], dz_r.at[s, k - 1], (fpeer(k), r, t))
        for a in range(2):
            send(dpiece(p, f, r), dp_s.at[s, a, 0], dp_r.at[s, a, 0], (f, across[a], t))
        square = direction.astype(F32)
        square = square * square
        square = jnp.sum(square.reshape(low_rows // 8, 8, width), axis=0)
        sums[p] = square
    for k in range(1, nf):
        send(sums, sz_s.at[k - 1], sz_r.at[k - 1], (fpeer(k), r, t), dst=sums_z.at[k - 1])
    relay("directions")
    for s, p in enumerate(order):
        for k in range(1, nf):
            src = fpeer(nf - k)
            arrived(dpiece(p, src, r), dz_s.at[s, k - 1], dz_r.at[s, k - 1])
            for a in range(2):
                send(dpiece(p, src, r), dp_s.at[s, a, k], dp_r.at[s, a, k], (f, across[a], t))
    for k in range(1, nf):
        arrived(sums_z.at[k - 1], sz_s.at[k - 1], sz_r.at[k - 1])
    total = sums[...]
    for k in range(1, nf):
        total = total + sums_z[k - 1]
    sums_r[0] = total
    for j in range(1, nr):
        send(sums_r.at[0], sr_s.at[j - 1], sr_r.at[j - 1], (f, rpeer(j), t), dst=sums_r.at[j])
    for s, p in enumerate(order):
        for k in range(nf):
            src = fpeer(nf - k) if k else f
            for a in range(2):
                arrived(dpiece(p, src, across[a]), dp_s.at[s, a, k], dp_r.at[s, a, k])
                send(
                    dpiece(p, src, across[a], a * low_half, low_half), dd_s.at[s, a, k], dd_r.at[s, a, k],
                    (f, across[1 - a], t),
                )
    for j in range(1, nr):
        send(low.at[:, :, lane], lw_s.at[j - 1], lw_r.at[j - 1], (f, rpeer(j), t))
    for j in range(1, nr):
        arrived(sums_r.at[j], sr_s.at[j - 1], sr_r.at[j - 1])
    total = sums_r[0]
    for j in range(1, nr):
        total = total + sums_r[j]
    sums_t[0] = total
    send(sums_t.at[0], st_s, st_r, sibling, dst=sums_t.at[1])
    arrived(fac.at[1 - t], fx_s, fx_r)
    put(fac, fac_out, out_sem.at[2])
    relay("gather")

    for s, p in enumerate(order):
        for k in range(nf):
            src = fpeer(nf - k) if k else f
            for a in range(2):
                arrived(dpiece(p, src, corner, a * low_half, low_half), dd_s.at[s, a, k], dd_r.at[s, a, k])
    put(dirs, dir_out, out_sem.at[3])
    arrived(sums_t.at[1], st_s, st_r)
    sum_out[...] = sums_t[0] + sums_t[1]
    for j in range(1, nr):
        rsrc = rpeer(nr - j)
        at = pl.ds(pl.multiple_of(rsrc * width, width), width)
        arrived(low.at[:, :, at], lw_s.at[j - 1], lw_r.at[j - 1])
    put(low, low_out, out_sem.at[4])
    for j, ch in relays:
        for d, (source, exists, _, _) in enumerate(line):
            piece = mpiece(mast, source(j), ch, other=True)
            arrived(piece, mp_s.at[d, j - 1, ch], mp_r.at[d, j - 1, ch], when=exists(j))
            put(piece, mpiece(mast_out, source(j), ch, other=True), op_sem.at[d, j - 1, ch], when=exists(j))
    for copy, when in outs:
        guarded(copy.wait, when)
    for copy, when in started:
        guarded(copy.wait_send, when)


def gather_all(nf, nr, normed_in, cotans, factors, firsts, seconds, masters):
    tokens, model = normed_in.shape
    cols = cotans[0].shape[1]
    rows, rank = factors[0].shape
    low_rows, width = rank // nf, cols // nr
    dma = pltpu.SemaphoreType.DMA
    anyspec = pl.BlockSpec(memory_space=pl.ANY)
    pair = lambda *shape: [dma(shape), dma(shape)]
    return pl.pallas_call(
        functools.partial(kernel, nf, nr),
        out_shape=(
            jax.ShapeDtypeStruct((2, model, rank), BF16),
            jax.ShapeDtypeStruct((2, rank, cols), BF16),
            jax.ShapeDtypeStruct((2, low_rows, cols), BF16),
            jax.ShapeDtypeStruct((2, model, cols), BF16),
            jax.ShapeDtypeStruct((2, 8, width), F32),
        ),
        in_specs=[anyspec] * 11,
        out_specs=(anyspec, anyspec, anyspec, anyspec, pl.BlockSpec(memory_space=pltpu.VMEM)),
        scratch_shapes=[
            pltpu.VMEM((tokens, model), BF16),
            pltpu.VMEM((2, tokens, cols), BF16),
            pltpu.VMEM((2, model, rank), BF16),
            pltpu.VMEM((tokens, rank), F32),
            pltpu.VMEM((2, rank, tokens), BF16),
            pltpu.VMEM((2, 6, rank // 2, width), BF16),
            pltpu.VMEM((2, 6, rank // 2, width), BF16),
            pltpu.VMEM((2, 2, rank // 2, width), F32),
            pltpu.VMEM((2, rank, width), F32),
            pltpu.VMEM((2, rank, width), BF16),
            pltpu.VMEM((2, nf - 1, low_rows, width), BF16),
            pltpu.VMEM((2, low_rows, width), F32),
            pltpu.VMEM((2, low_rows, width), F32),
            pltpu.VMEM((2, low_rows, cols), BF16),
            pltpu.VMEM((2, rank, cols), BF16),
            pltpu.VMEM((2, rows, cols), F32),
            pltpu.VMEM((2, model, cols), BF16),
            pltpu.VMEM((2, 8, width), F32),
            pltpu.VMEM((nf - 1, 2, 8, width), F32),
            pltpu.VMEM((nr, 2, 8, width), F32),
            pltpu.VMEM((2, 2, 8, width), F32),
            dma((10,)),
            dma((5,)),
            dma((2, nf - 1, CHUNKS)),
            dma((2, nf - 1, CHUNKS)),
            *pair(nf - 1),
            *pair(2, nf - 1),
            *pair(2, nf - 1),
            dma,
            dma,
            *pair(TOKEN_TILES),
            *pair(2, 6),
            *pair(2, nf - 1),
            *pair(2, nf - 1),
            *pair(2, 2, nf),
            *pair(2, 2, nf),
            *pair(nr - 1),
            *pair(nf - 1),
            *pair(nr - 1),
            dma,
            dma,
            *pair(2, nf - 1, CHUNKS),
            *pair(2, nf - 1, CHUNKS),
        ],
        cost_estimate=pl.CostEstimate(
            flops=10 * tokens * model * rank, bytes_accessed=400 * 2**20, transcendentals=0
        ),
        compiler_params=pltpu.CompilerParams(
            collective_id=0, has_side_effects=True, vmem_limit_bytes=60 * 2**20
        ),
    )(normed_in, *cotans, *factors, *firsts, *seconds, *masters)


def finish_kernel(
    nf,
    entries,
    where,
    scales,
    fac_hbm,
    dir_hbm,
    low_hbm,
    mast_hbm,
    first0,
    first1,
    second0,
    second1,
    upd0,
    upd1,
    nfirst0,
    nfirst1,
    nsecond0,
    nsecond1,
    copy0,
    copy1,
    fac,
    dirs,
    low,
    mast,
    upd,
    moments,
    fac_sem,
    mast_sem,
    dir_sem,
    mom_sem,
    copy_sem,
    upd_sem,
    mout_sem,
):
    f = where[0]
    model = mast.shape[1]
    rows = model // nf
    unit = min(rows, 256)
    per = rows // unit
    units = [(p, i, u) for p in range(2) for i in range(nf) for u in range(per)]

    def span(i, u):
        return pl.ds(pl.multiple_of(lax.rem(f + i, nf) * rows + u * unit, unit), unit)

    def load(n):
        p, i, u = units[n]
        return (
            pltpu.make_async_copy(fac_hbm.at[p, span(i, u), :], fac.at[p, span(i, u), :], fac_sem.at[n]),
            pltpu.make_async_copy(mast_hbm.at[p, span(i, u), :], mast.at[p, span(i, u), :], mast_sem.at[n]),
        )

    load_d = [pltpu.make_async_copy(dir_hbm.at[p], dirs.at[p], dir_sem.at[p]) for p in range(2)]
    loads = [load(n) for n in range(len(units))]
    load_m = [
        pltpu.make_async_copy(src, moments.at[i], mom_sem.at[i])
        for i, src in enumerate((first0, first1, second0, second1))
    ]
    load_l = pltpu.make_async_copy(low_hbm, low, mom_sem.at[4])
    load_d[0].start()
    for n, pair in enumerate(loads):
        for copy in pair:
            copy.start()
        if n == 1:
            load_d[1].start()
    for copy in (load_l, *load_m):
        copy.start()
    outs = []

    def put(src, dst, sem):
        copy = pltpu.make_async_copy(src, dst, sem)
        copy.start()
        outs.append(copy)

    for n, (p, i, u) in enumerate(units):
        if i == 0 and u == 0:
            load_d[p].wait()
        for copy in loads[n]:
            copy.wait()
        update = jnp.dot(fac[p, span(i, u), :], dirs[p], preferred_element_type=F32) * scales[p]
        if i == 0:
            upd[p, u * unit:(u + 1) * unit, :] = update
            put(
                upd.at[p, pl.ds(u * unit, unit), :], (upd0, upd1)[p].at[pl.ds(u * unit, unit), :],
                upd_sem.at[p, u],
            )
        mast[p, span(i, u), :] = (mast[p, span(i, u), :].astype(F32) - step_rate * update).astype(BF16)
        put(mast.at[p, span(i, u), :], (copy0, copy1)[p].at[span(i, u), :], copy_sem.at[n])
    load_l.wait()
    for copy in load_m:
        copy.wait()
    for p in range(2):
        again = low[p].astype(F32)
        moments[p] = beta_first * moments[p] + (1.0 - beta_first) * again
        put(moments.at[p], (nfirst0, nfirst1)[p], mout_sem.at[p])
        moments[2 + p] = beta_second * moments[2 + p] + (1.0 - beta_second) * again * again
        put(moments.at[2 + p], (nsecond0, nsecond1)[p], mout_sem.at[2 + p])
    for copy in outs:
        copy.wait()


def finish(nf, entries, where, scales, fac, dirs, low, mast, firsts, seconds):
    _, model, rank = fac.shape
    cols = dirs.shape[2]
    rows, low_rows = model // nf, low.shape[1]
    unit = min(rows, 256)
    count = 2 * (model // unit)
    dma = pltpu.SemaphoreType.DMA
    anyspec = pl.BlockSpec(memory_space=pl.ANY)
    smem = pl.BlockSpec(memory_space=pltpu.SMEM)
    shape = jax.ShapeDtypeStruct
    return pl.pallas_call(
        functools.partial(finish_kernel, nf, entries),
        out_shape=(
            *[shape((rows, cols), F32)] * 2,
            *[shape((low_rows, cols), F32)] * 4,
            *[shape((model, cols), BF16)] * 2,
        ),
        in_specs=[smem, smem] + [anyspec] * 8,
        out_specs=(anyspec,) * 8,
        scratch_shapes=[
            pltpu.VMEM((2, model, rank), BF16),
            pltpu.VMEM((2, rank, cols), BF16),
            pltpu.VMEM((2, low_rows, cols), BF16),
            pltpu.VMEM((2, model, cols), BF16),
            pltpu.VMEM((2, rows, cols), F32),
            pltpu.VMEM((4, low_rows, cols), F32),
            dma((count,)),
            dma((count,)),
            dma((2,)),
            dma((5,)),
            dma((count,)),
            dma((2, rows // unit)),
            dma((4,)),
        ],
        cost_estimate=pl.CostEstimate(
            flops=4 * model * rank * cols, bytes_accessed=30 * 2**20, transcendentals=0
        ),
        compiler_params=pltpu.CompilerParams(vmem_limit_bytes=60 * 2**20),
    )(where, scales, fac, dirs, low, mast, *firsts, *seconds)


def body(
    nf,
    nr,
    nt,
    normed_in,
    cotan_rec,
    cotan_gate,
    factor_rec,
    factor_gate,
    first_rec,
    first_gate,
    second_rec,
    second_gate,
    master_rec,
    master_gate,
):
    factors = (factor_rec, factor_gate)
    firsts = (first_rec, first_gate)
    seconds = (second_rec, second_gate)
    fac, dirs, low, mast, sums = gather_all(
        nf, nr, normed_in, (cotan_rec, cotan_gate), factors, firsts, seconds, (master_rec, master_gate)
    )
    entries = float(dirs.shape[1] * dirs.shape[2] * nt)
    scales = 1.0 / jnp.sqrt(jnp.sum(sums, axis=(1, 2)) / entries + scale_floor)
    where = lax.axis_index("fs").astype(jnp.int32).reshape(1)
    return finish(nf, entries, where, scales, fac, dirs, low, mast, firsts, seconds)


def solution(mesh):
    nf, nr, nt = mesh.shape["fs"], mesh.shape["rep"], mesh.shape["tp"]
    rows = P("fs", "tp")
    return jax.shard_map(
        functools.partial(body, nf, nr, nt),
        mesh=mesh,
        in_specs=(
            P(("fs", "rep"), None),
            P(("fs", "rep"), "tp"),
            P(("fs", "rep"), "tp"),
            P("fs", None),
            P("fs", None),
            *[rows] * 6,
        ),
        out_specs=(*[rows] * 6, P(None, "tp"), P(None, "tp")),
        check_vma=False,
    )
```

time: 188 us -> 143 us (0.76)
  the two profiles are of different devices: /device:TPU:0 before, /device:TPU:26 now
where the time goes in v1:
time: 143 us; the launch traced here: 142 us
  Pallas kernels  140 us (98%)
    pallas_call x1, Pallas kernels, gather_all(): pl.pallas_call(functools.partial(kernel, nf, nr), out_shape=(jax.ShapeDty...  125 us
    pallas_call x1, Pallas kernels, finish(): pl.pallas_call(functools.partial(finish_kernel, nf, entries), out_shape=(...  14.9 us

profile of v1, /device:TPU:26, one launch (start us, length us, event | category | flops | bytes accessed | tf_op | source)
XLA Modules:
  0.0 142.4 jit_solution(7309011708496432228)
XLA Ops:
  0.6 125.5 %shard_map.170 = (bf16[2,2048,512]{2,1,0:T(8,128)(2,1)}, bf16[2,512,1024]{2,1,0:T(8,128)(2,1)}, bf16[2,128,1024]{2,1,0:T(8,128)(2,1)}, bf16[2,2048,1024]{2,1,0:T(8,128)(2,1)}, f32[2,8,256]{2,1,0:T(8,128)}) custom-call(bf16[1536,2048]{1,0:T(8,128)(2,1)} %x_hbm.1, bf16[1536,1024]{1,0:T(8,128)(2,1)} %c0_hbm.1, bf16[1536,1024]{1,0:T(8,128)(2,1)} %c1_hbm.1, ...), custom_call_target="tpu_custom_call" | custom-call | flops 16106127360 | bytes 419430400 | tf_op jit(solution)/shard_map/pallas_call | solution.py:439
  126.1 0.8 reduce_sum.9
  127.0 0.6 add_rsqrt_fusion.scales
  127.5 14.9 %shard_map.171 = (f32[512,1024]{1,0:T(8,128)}, f32[512,1024]{1,0:T(8,128)}, f32[128,1024]{1,0:T(8,128)}, f32[128,1024]{1,0:T(8,128)}, f32[128,1024]{1,0:T(8,128)...) custom-call(s32[1]{0:T(128)} %bitcast.where, f32[2]{0:T(128)} %add_rsqrt_fusion.scales, ...), custom_call_target="tpu_custom_call" | custom-call | flops 4294967296 | bytes 31457280 | tf_op jit(solution)/shard_map/pallas_call | solution.py:615

commit v2 on v1

--- a/solution.py
+++ b/solution.py
@@ -19,19 +19,21 @@
 HALF_CHUNKS = 2
 CHUNKS = 2 * HALF_CHUNKS
 SHARES = {
-    "factors": 0.0,
-    "projection": 0.0,
-    "products": 0.17,
-    "stage": 0.34,
-    "reduce": 0.42,
-    "directions": 0.5,
-    "gather": 1.0,
+    "projection": (0.0, 0.17, 0.08, 0.0),
+    "products": (0.0, 0.25, 0.08, 0.0),
+    "stage": (0.0, 0.33, 0.08, 0.0),
+    "reduce": (0.5, 0.42, 0.17, 0.33),
+    "directions": (0.5, 0.42, 0.17, 0.33),
+    "gather_z": (0.67, 0.5, 0.33, 0.33),
+    "gather": (0.83, 0.67, 0.67, 0.67),
+    "end": (1.0, 1.0, 1.0, 1.0),
 }
 
 
 def kernel(
     nf,
     nr,
+    entries,
     x_hbm,
     c0_hbm,
     c1_hbm,
@@ -43,11 +45,9 @@
     second1,
     mast0_hbm,
     mast1_hbm,
-    fac_out,
-    dir_out,
-    low_out,
-    mast_out,
-    sum_out,
+    fresh,
+    upd,
+    moments,
     x,
     c,
     fac,
@@ -59,20 +59,14 @@
     own,
     mid,
     recv_fs,
-    fst,
-    snd,
     low,
     dirs,
-    wide,
     mast,
     sums,
     sums_z,
     sums_r,
     sums_t,
     local_sem,
-    out_sem,
-    oz_sem,
-    op_sem,
     fz_s,
     fz_r,
     fp_s,
@@ -141,8 +135,8 @@
         pltpu.make_async_copy(fac1_hbm, mine, local_sem.at[0]).start()
 
     load_m = [
-        pltpu.make_async_copy(mast0_hbm, wide.at[0], local_sem.at[8]),
-        pltpu.make_async_copy(mast1_hbm, wide.at[1], local_sem.at[9]),
+        pltpu.make_async_copy(mast0_hbm, upd.at[0], local_sem.at[8]),
+        pltpu.make_async_copy(mast1_hbm, upd.at[1], local_sem.at[9]),
     ]
     load_x = pltpu.make_async_copy(x_hbm, x, local_sem.at[1])
     for load in (*load_m, load_x):
@@ -152,11 +146,10 @@
         pltpu.make_async_copy(c1_hbm, c.at[1], local_sem.at[3]),
     ]
     lane = pl.ds(pl.multiple_of(r * width, width), width)
-    load_s = []
-    for i, (src, dst) in enumerate(
-        ((first0, fst.at[0]), (first1, fst.at[1]), (second0, snd.at[0]), (second1, snd.at[1]))
-    ):
-        load_s.append(pltpu.make_async_copy(src.at[:, lane], dst, local_sem.at[4 + i]))
+    load_s = [
+        pltpu.make_async_copy(src, moments.at[i], local_sem.at[4 + i])
+        for i, src in enumerate((first0, first1, second0, second1))
+    ]
     for load in (*load_c, *load_s):
         load.start()
 
@@ -190,13 +183,6 @@
     def arrived(ref, s_sem, r_sem, when=None):
         guarded(remote(ref, ref, s_sem, r_sem, sibling).wait_recv, when)
 
-    outs = []
-
-    def put(src, dst, sem, when=None):
-        copy = pltpu.make_async_copy(src, dst, sem)
-        guarded(copy.start, when)
-        outs.append((copy, when))
-
     def fpiece(ff, rr, start=0, count=quarter):
         at = pl.multiple_of(ff * rows + rr * quarter + start, count)
         return fac.at[t, pl.ds(at, count), :]
@@ -211,37 +197,93 @@
         (lambda j: lax.rem(f + j, nf), lambda j: f < nf - j, fpeer(nf - 1), f > 0),
     )
 
-    def mpiece(ref, ff, ch, other=False):
-        p = ch % 2
-        h = rx if p == 0 else ry
+    def mrange(ff, ch, other=False):
+        h = rx if ch % 2 == 0 else ry
         if other:
             h = 1 - h
-        at = pl.multiple_of(ff * rows + h * half + (ch // 2) * chunk, chunk)
-        return ref.at[p, pl.ds(at, chunk), :]
+        return ff * rows + h * half + (ch // 2) * chunk, chunk
+
+    def mpiece(ff, ch, other=False):
+        start, count = mrange(ff, ch, other)
+        return mast.at[ch % 2, pl.ds(pl.multiple_of(start, count), count), :]
+
+    def my_turn(ch):
+        return (ry if ch % 2 == 0 else rx) == ch // 2
+
+    def swap():
+        for d, (source, exists, _, there) in enumerate(line):
+            for ch in range(CHUNKS):
+                piece = mpiece(source(1), ch)
+                mine_first = exists(1) & jnp.logical_not(there) & my_turn(ch)
+                arrived(piece, mz_s.at[d, 0, ch], mz_r.at[d, 0, ch], when=mine_first)
+                send(
+                    piece, mz_s.at[d, 1, ch], mz_r.at[d, 0, ch], (f, across[1 - ch % 2], t),
+                    when=mine_first,
+                )
 
     for p in range(2):
         load_m[p].wait()
-        mast[p, block(f), :] = wide[p].astype(BF16)
+        mast[p, block(f), :] = upd[p].astype(BF16)
     for ch in range(CHUNKS):
         for d, (_, _, onto, there) in enumerate(line):
-            send(mpiece(mast, f, ch), mz_s.at[d, 0, ch], mz_r.at[d, 0, ch], (onto, r, t), when=there)
-    for p in range(2):
-        put(mast.at[p, block(f), :], mast_out.at[p, block(f), :], out_sem.at[p])
+            to_end = f == (nf - 2 if d == 0 else 1)
+            send(
+                mpiece(f, ch), mz_s.at[d, 0, ch], mz_r.at[d, 0, ch], (onto, r, t),
+                when=there & (jnp.logical_not(to_end) | my_turn(ch)),
+            )
 
     relays = [(j, ch) for j in range(1, nf) for ch in range(CHUNKS)]
-    done = [0]
+    done = [0, 0, 0, 0]
+    last = jnp.logical_or(f == 0, f == nf - 1)
+    inner = jnp.logical_not(last)
+
+    def land(j, ch, when, swapped=False):
+        for d, (source, exists, _, there) in enumerate(line):
+            due = exists(j) & when
+            if j == 1:
+                due = due & (jnp.logical_not(there | my_turn(ch)) if swapped else there)
+            elif swapped:
+                continue
+            piece = mpiece(source(j), ch)
+            arrived(piece, mz_s.at[d, j - 1, ch], mz_r.at[d, j - 1, ch], when=due)
+
+    def onward(j, ch, ending):
+        if j == nf - 1:
+            return
+        for d, (source, exists, onto, there) in enumerate(line):
+            to_end = f == (nf - 2 if d == 0 else 1)
+            if not ending:
+                to_end = jnp.logical_not(to_end)
+            send(
+                mpiece(source(j), ch), mz_s.at[d, j, ch], mz_r.at[d, j, ch], (onto, r, t),
+                when=exists(j) & there & inner & to_end,
+            )
+
+    def aside(j, ch, when):
+        for d, (source, exists, _, _) in enumerate(line):
+            piece = mpiece(source(j), ch)
+            send(
+                piece, mp_s.at[d, j - 1, ch], mp_r.at[d, j - 1, ch], (f, across[ch % 2], t),
+                when=exists(j) & when,
+            )
 
     def relay(point):
-        upto = round(SHARES[point] * len(relays))
-        for j, ch in relays[done[0]:upto]:
-            for d, (source, exists, onto, there) in enumerate(line):
-                piece = mpiece(mast, source(j), ch)
-                arrived(piece, mz_s.at[d, j - 1, ch], mz_r.at[d, j - 1, ch], when=exists(j))
-                if j < nf - 1:
-                    send(piece, mz_s.at[d, j, ch], mz_r.at[d, j, ch], (onto, r, t), when=exists(j) & there)
-                send(piece, mp_s.at[d, j - 1, ch], mp_r.at[d, j - 1, ch], (f, across[ch % 2], t), when=exists(j))
-                put(piece, mpiece(mast_out, source(j), ch), oz_sem.at[d, j - 1, ch], when=exists(j))
-        done[0] = max(done[0], upto)
+        ends = [max(d, round(share * len(relays))) for d, share in zip(done, SHARES[point])]
+        for n in range(done[0], ends[0]):
+            land(*relays[n], last)
+            land(*relays[n], last, swapped=True)
+            aside(*relays[n], last)
+        landed = max(done[1:])
+        for n in range(min(done[1:]), max(ends[1:])):
+            if n >= landed:
+                land(*relays[n], inner)
+            if done[1] <= n < ends[1]:
+                onward(*relays[n], True)
+            if done[2] <= n < ends[2]:
+                onward(*relays[n], False)
+            if done[3] <= n < ends[3]:
+                aside(*relays[n], inner)
+        done[:] = ends
 
     def project(ff, first=False):
         at = block(ff)
@@ -267,13 +309,17 @@
                 fpiece(src, across[a], a * fhalf, fhalf), fd_s.at[a, k - 1], fd_r.at[a, k - 1],
                 (f, across[1 - a], t),
             )
-    relay("factors")
-    for k in range(1, nf):
-        src = fpeer(nf - k)
-        for a in range(2):
-            arrived(fpiece(src, corner, a * fhalf, fhalf), fd_s.at[a, k - 1], fd_r.at[a, k - 1])
-        if k < nf - 1:
-            project(src)
+    def corner_arrived(k):
+        for a in range(2):
+            piece = fpiece(fpeer(nf - k), corner, a * fhalf, fhalf)
+            arrived(piece, fd_s.at[a, k - 1], fd_r.at[a, k - 1])
+
+    @pl.loop(1, nf - 1)
+    def _(k):
+        corner_arrived(k)
+        project(fpeer(nf - k))
+
+    corner_arrived(nf - 1)
     at = block(fpeer(1))
     for i in range(TOKEN_TILES):
         span = pl.ds(i * tile, tile)
@@ -324,6 +370,7 @@
             got_part(s, a)
             part[s, 4 + a] = (keep[s, a] + recv[s, a].astype(F32)).astype(BF16)
             pass_part(s, 4 + a, 1 - a)
+    swap()
     relay("stage")
     for s in range(2):
         for a in range(2):
@@ -353,8 +400,8 @@
         rounded = total.astype(BF16)
         low[p, :, lane] = rounded
         again = rounded.astype(F32)
-        new_first = beta_first * fst[p] + (1.0 - beta_first) * again
-        new_second = beta_second * snd[p] + (1.0 - beta_second) * again * again
+        new_first = beta_first * moments[p, :, lane] + (1.0 - beta_first) * again
+        new_second = beta_second * moments[2 + p, :, lane] + (1.0 - beta_second) * again * again
         direction = (new_first / jnp.sqrt(new_second)).astype(BF16)
         dirs[p, rank_rows(f), lane] = direction
         for k in range(1, nf):
@@ -374,6 +421,7 @@
             arrived(dpiece(p, src, r), dz_s.at[s, k - 1], dz_r.at[s, k - 1])
             for a in range(2):
                 send(dpiece(p, src, r), dp_s.at[s, a, k], dp_r.at[s, a, k], (f, across[a], t))
+    relay("gather_z")
     for k in range(1, nf):
         arrived(sums_z.at[k - 1], sz_s.at[k - 1], sz_r.at[k - 1])
     total = sums[...]
@@ -401,7 +449,6 @@
     sums_t[0] = total
     send(sums_t.at[0], st_s, st_r, sibling, dst=sums_t.at[1])
     arrived(fac.at[1 - t], fx_s, fx_r)
-    put(fac, fac_out, out_sem.at[2])
     relay("gather")
 
     for s, p in enumerate(order):
@@ -409,26 +456,68 @@
             src = fpeer(nf - k) if k else f
             for a in range(2):
                 arrived(dpiece(p, src, corner, a * low_half, low_half), dd_s.at[s, a, k], dd_r.at[s, a, k])
-    put(dirs, dir_out, out_sem.at[3])
+    relay("end")
     arrived(sums_t.at[1], st_s, st_r)
-    sum_out[...] = sums_t[0] + sums_t[1]
+    total = sums_t[0] + sums_t[1]
+    scales = [1.0 / jnp.sqrt(jnp.sum(total[p]) / entries + scale_floor) for p in range(2)]
+
+    def update_of(p, at):
+        return jnp.dot(fac[p, at, :], dirs[p], preferred_element_type=F32) * scales[p]
+
+    def renew(p, start, count):
+        at = pl.ds(pl.multiple_of(start, count), count)
+        fresh[p, at, :] = (mast[p, at, :].astype(F32) - step_rate * update_of(p, at)).astype(BF16)
+
+    unit = min(rows, 256)
+
+    def renew_block(ff):
+        for p in range(2):
+            for i in range(rows // unit):
+                renew(p, ff * rows + i * unit, unit)
+
+    for p in range(2):
+        for i in range(rows // unit):
+            at = pl.ds(pl.multiple_of(f * rows + i * unit, unit), unit)
+            update = update_of(p, at)
+            span = pl.ds(i * unit, unit)
+            fresh[p, at, :] = (mast[p, at, :].astype(F32) - step_rate * update).astype(BF16)
+            upd[p, span, :] = update
     for j in range(1, nr):
         rsrc = rpeer(nr - j)
         at = pl.ds(pl.multiple_of(rsrc * width, width), width)
         arrived(low.at[:, :, at], lw_s.at[j - 1], lw_r.at[j - 1])
-    put(low, low_out, out_sem.at[4])
-    for j, ch in relays:
+    for p in range(2):
+        again = low[p].astype(F32)
+        moments[p] = beta_first * moments[p] + (1.0 - beta_first) * again
+        moments[2 + p] = beta_second * moments[2 + p] + (1.0 - beta_second) * again * again
+
+    def beside(j, ch, d):
+        source, exists, _, _ = line[d]
+        piece = mpiece(source(j), ch, other=True)
+        arrived(piece, mp_s.at[d, j - 1, ch], mp_r.at[d, j - 1, ch], when=exists(j))
+
+    @pl.loop(1, nf - 1)
+    def _(j):
         for d, (source, exists, _, _) in enumerate(line):
-            piece = mpiece(mast, source(j), ch, other=True)
-            arrived(piece, mp_s.at[d, j - 1, ch], mp_r.at[d, j - 1, ch], when=exists(j))
-            put(piece, mpiece(mast_out, source(j), ch, other=True), op_sem.at[d, j - 1, ch], when=exists(j))
-    for copy, when in outs:
-        guarded(copy.wait, when)
+            for ch in range(CHUNKS):
+                beside(j, ch, d)
+            guarded(lambda: renew_block(source(j)), exists(j))
+
+    j = nf - 1
+    for ch in range(CHUNKS):
+        for d, (source, exists, _, _) in enumerate(line):
+            start, count = mrange(source(j), ch)
+            guarded(lambda: renew(ch % 2, start, count), exists(j))
+    for ch in range(CHUNKS):
+        for d, (source, exists, _, _) in enumerate(line):
+            beside(j, ch, d)
+            start, count = mrange(source(j), ch, other=True)
+            guarded(lambda: renew(ch % 2, start, count), exists(j))
     for copy, when in started:
         guarded(copy.wait_send, when)
 
 
-def gather_all(nf, nr, normed_in, cotans, factors, firsts, seconds, masters):
+def gather_all(nf, nr, entries, normed_in, cotans, factors, firsts, seconds, masters):
     tokens, model = normed_in.shape
     cols = cotans[0].shape[1]
     rows, rank = factors[0].shape
@@ -437,16 +526,14 @@
     anyspec = pl.BlockSpec(memory_space=pl.ANY)
     pair = lambda *shape: [dma(shape), dma(shape)]
     return pl.pallas_call(
-        functools.partial(kernel, nf, nr),
+        functools.partial(kernel, nf, nr, entries),
         out_shape=(
-            jax.ShapeDtypeStruct((2, model, rank), BF16),
-            jax.ShapeDtypeStruct((2, rank, cols), BF16),
-            jax.ShapeDtypeStruct((2, low_rows, cols), BF16),
-            jax.ShapeDtypeStruct((2, model, cols), BF16),
-            jax.ShapeDtypeStruct((2, 8, width), F32),
+            pltpu.VMEM((2, model, cols), BF16),
+            pltpu.VMEM((2, rows, cols), F32),
+            pltpu.VMEM((4, low_rows, cols), F32),
         ),
         in_specs=[anyspec] * 11,
-        out_specs=(anyspec, anyspec, anyspec, anyspec, pl.BlockSpec(memory_space=pltpu.VMEM)),
+        out_specs=(pl.BlockSpec(memory_space=pltpu.VMEM),) * 3,
         scratch_shapes=[
             pltpu.VMEM((tokens, model), BF16),
             pltpu.VMEM((2, tokens, cols), BF16),
@@ -459,20 +546,14 @@
             pltpu.VMEM((2, rank, width), F32),
             pltpu.VMEM((2, rank, width), BF16),
             pltpu.VMEM((2, nf - 1, low_rows, width), BF16),
-            pltpu.VMEM((2, low_rows, width), F32),
-            pltpu.VMEM((2, low_rows, width), F32),
             pltpu.VMEM((2, low_rows, cols), BF16),
             pltpu.VMEM((2, rank, cols), BF16),
-            pltpu.VMEM((2, rows, cols), F32),
             pltpu.VMEM((2, model, cols), BF16),
             pltpu.VMEM((2, 8, width), F32),
             pltpu.VMEM((nf - 1, 2, 8, width), F32),
             pltpu.VMEM((nr, 2, 8, width), F32),
             pltpu.VMEM((2, 2, 8, width), F32),
             dma((10,)),
-            dma((5,)),
-            dma((2, nf - 1, CHUNKS)),
-            dma((2, nf - 1, CHUNKS)),
             *pair(nf - 1),
             *pair(2, nf - 1),
             *pair(2, nf - 1),
@@ -496,151 +577,43 @@
             flops=10 * tokens * model * rank, bytes_accessed=400 * 2**20, transcendentals=0
         ),
         compiler_params=pltpu.CompilerParams(
-            collective_id=0, has_side_effects=True, vmem_limit_bytes=60 * 2**20
+            collective_id=0, has_side_effects=True, vmem_limit_bytes=46 * 2**20
         ),
     )(normed_in, *cotans, *factors, *firsts, *seconds, *masters)
 
 
-def finish_kernel(
-    nf,
-    entries,
-    where,
-    scales,
-    fac_hbm,
-    dir_hbm,
-    low_hbm,
-    mast_hbm,
-    first0,
-    first1,
-    second0,
-    second1,
-    upd0,
-    upd1,
-    nfirst0,
-    nfirst1,
-    nsecond0,
-    nsecond1,
-    copy0,
-    copy1,
-    fac,
-    dirs,
-    low,
-    mast,
-    upd,
-    moments,
-    fac_sem,
-    mast_sem,
-    dir_sem,
-    mom_sem,
-    copy_sem,
-    upd_sem,
-    mout_sem,
-):
-    f = where[0]
-    model = mast.shape[1]
-    rows = model // nf
-    unit = min(rows, 256)
-    per = rows // unit
-    units = [(p, i, u) for p in range(2) for i in range(nf) for u in range(per)]
-
-    def span(i, u):
-        return pl.ds(pl.multiple_of(lax.rem(f + i, nf) * rows + u * unit, unit), unit)
-
-    def load(n):
-        p, i, u = units[n]
-        return (
-            pltpu.make_async_copy(fac_hbm.at[p, span(i, u), :], fac.at[p, span(i, u), :], fac_sem.at[n]),
-            pltpu.make_async_copy(mast_hbm.at[p, span(i, u), :], mast.at[p, span(i, u), :], mast_sem.at[n]),
-        )
-
-    load_d = [pltpu.make_async_copy(dir_hbm.at[p], dirs.at[p], dir_sem.at[p]) for p in range(2)]
-    loads = [load(n) for n in range(len(units))]
-    load_m = [
-        pltpu.make_async_copy(src, moments.at[i], mom_sem.at[i])
-        for i, src in enumerate((first0, first1, second0, second1))
-    ]
-    load_l = pltpu.make_async_copy(low_hbm, low, mom_sem.at[4])
-    load_d[0].start()
-    for n, pair in enumerate(loads):
-        for copy in pair:
-            copy.start()
-        if n == 1:
-            load_d[1].start()
-    for copy in (load_l, *load_m):
+def finish_kernel(fresh, upd, moments, *rest):
+    outs, sem = rest[:-1], rest[-1]
+    pieces = [(upd.at[p], outs[p]) for p in range(2)]
+    pieces += [(moments.at[i], outs[2 + i]) for i in range(4)]
+    share = fresh.shape[1] // 4
+    for p in range(2):
+        for i in range(4):
+            span = pl.ds(i * share, share)
+            pieces.append((fresh.at[p, span, :], outs[6 + p].at[span, :]))
+    copies = [pltpu.make_async_copy(src, dst, sem.at[i]) for i, (src, dst) in enumerate(pieces)]
+    for copy in copies:
         copy.start()
-    outs = []
-
-    def put(src, dst, sem):
-        copy = pltpu.make_async_copy(src, dst, sem)
-        copy.start()
-        outs.append(copy)
-
-    for n, (p, i, u) in enumerate(units):
-        if i == 0 and u == 0:
-            load_d[p].wait()
-        for copy in loads[n]:
-            copy.wait()
-        update = jnp.dot(fac[p, span(i, u), :], dirs[p], preferred_element_type=F32) * scales[p]
-        if i == 0:
-            upd[p, u * unit:(u + 1) * unit, :] = update
-            put(
-                upd.at[p, pl.ds(u * unit, unit), :], (upd0, upd1)[p].at[pl.ds(u * unit, unit), :],
-                upd_sem.at[p, u],
-            )
-        mast[p, span(i, u), :] = (mast[p, span(i, u), :].astype(F32) - step_rate * update).astype(BF16)
-        put(mast.at[p, span(i, u), :], (copy0, copy1)[p].at[span(i, u), :], copy_sem.at[n])
-    load_l.wait()
-    for copy in load_m:
+    for copy in copies:
         copy.wait()
-    for p in range(2):
-        again = low[p].astype(F32)
-        moments[p] = beta_first * moments[p] + (1.0 - beta_first) * again
-        put(moments.at[p], (nfirst0, nfirst1)[p], mout_sem.at[p])
-        moments[2 + p] = beta_second * moments[2 + p] + (1.0 - beta_second) * again * again
-        put(moments.at[2 + p], (nsecond0, nsecond1)[p], mout_sem.at[2 + p])
-    for copy in outs:
-        copy.wait()
-
-
-def finish(nf, entries, where, scales, fac, dirs, low, mast, firsts, seconds):
-    _, model, rank = fac.shape
-    cols = dirs.shape[2]
-    rows, low_rows = model // nf, low.shape[1]
-    unit = min(rows, 256)
-    count = 2 * (model // unit)
-    dma = pltpu.SemaphoreType.DMA
+
+
+def finish(fresh, upd, moments):
+    shape = jax.ShapeDtypeStruct
     anyspec = pl.BlockSpec(memory_space=pl.ANY)
-    smem = pl.BlockSpec(memory_space=pltpu.SMEM)
-    shape = jax.ShapeDtypeStruct
     return pl.pallas_call(
-        functools.partial(finish_kernel, nf, entries),
+        finish_kernel,
         out_shape=(
-            *[shape((rows, cols), F32)] * 2,
-            *[shape((low_rows, cols), F32)] * 4,
-            *[shape((model, cols), BF16)] * 2,
+            *[shape(upd.shape[1:], F32)] * 2,
+            *[shape(moments.shape[1:], F32)] * 4,
+            *[shape(fresh.shape[1:], BF16)] * 2,
         ),
-        in_specs=[smem, smem] + [anyspec] * 8,
+        in_specs=[pl.BlockSpec(memory_space=pltpu.VMEM)] * 3,
         out_specs=(anyspec,) * 8,
-        scratch_shapes=[
-            pltpu.VMEM((2, model, rank), BF16),
-            pltpu.VMEM((2, rank, cols), BF16),
-            pltpu.VMEM((2, low_rows, cols), BF16),
-            pltpu.VMEM((2, model, cols), BF16),
-            pltpu.VMEM((2, rows, cols), F32),
-            pltpu.VMEM((4, low_rows, cols), F32),
-            dma((count,)),
-            dma((count,)),
-            dma((2,)),
-            dma((5,)),
-            dma((count,)),
-            dma((2, rows // unit)),
-            dma((4,)),
-        ],
-        cost_estimate=pl.CostEstimate(
-            flops=4 * model * rank * cols, bytes_accessed=30 * 2**20, transcendentals=0
-        ),
-        compiler_params=pltpu.CompilerParams(vmem_limit_bytes=60 * 2**20),
-    )(where, scales, fac, dirs, low, mast, *firsts, *seconds)
+        scratch_shapes=[pltpu.SemaphoreType.DMA((14,))],
+        cost_estimate=pl.CostEstimate(flops=0, bytes_accessed=14 * 2**20, transcendentals=0),
+        compiler_params=pltpu.CompilerParams(vmem_limit_bytes=2**20),
+    )(fresh, upd, moments)
 
 
 def body(
@@ -662,13 +635,13 @@
     factors = (factor_rec, factor_gate)
     firsts = (first_rec, first_gate)
     seconds = (second_rec, second_gate)
-    fac, dirs, low, mast, sums = gather_all(
-        nf, nr, normed_in, (cotan_rec, cotan_gate), factors, firsts, seconds, (master_rec, master_gate)
+    entries = float(factor_rec.shape[1] * cotan_rec.shape[1] * nt)
+    return finish(
+        *gather_all(
+            nf, nr, entries, normed_in, (cotan_rec, cotan_gate), factors, firsts, seconds,
+            (master_rec, master_gate),
+        )
     )
-    entries = float(dirs.shape[1] * dirs.shape[2] * nt)
-    scales = 1.0 / jnp.sqrt(jnp.sum(sums, axis=(1, 2)) / entries + scale_floor)
-    where = lax.axis_index("fs").astype(jnp.int32).reshape(1)
-    return finish(nf, entries, where, scales, fac, dirs, low, mast, firsts, seconds)
 
 
 def solution(mesh):

time: 143 us -> 119 us (0.83)
  the two profiles are of different devices: /device:TPU:26 before, /device:TPU:0 now
where the time goes in v2:
time: 119 us
  Pallas kernels  118 us (99%)
    pallas_call x1, Pallas kernels, gather_all(): pl.pallas_call(functools.partial(kernel, nf, nr, entries), out_shape=(plt...  113 us
    pallas_call x1, Pallas kernels, finish(): pl.pallas_call(finish_kernel, out_shape=(*[shape(upd.shape[1:], F32)] * 2...  5.31 us

profile of v2, /device:TPU:0, one launch (start us, length us, event | category | flops | bytes accessed | tf_op | source)
XLA Modules:
  0.0 118.9 jit_solution(10265509920205989176)
XLA Ops:
  0.6 112.8 %shard_map.170 = (bf16[2,2048,1024]{2,1,0:T(8,128)(2,1)S(1)}, f32[2,512,1024]{2,1,0:T(8,128)S(1)}, f32[4,128,1024]{2,1,0:T(8,128)S(1)}) custom-call(bf16[1536,2048]{1,0:T(8,128)(2,1)} %x_hbm.1, bf16[1536,1024]{1,0:T(8,128)(2,1)} %c0_hbm.1, bf16[1536,1024]{1,0:T(8,128)(2,1)} %c1_hbm.1, bf16[512,512]{1,0:T(8,128)(2,1)} %fac0_hbm.1, bf16[512,512]{1,0:T(8,128)(2,1)} %fac1_hbm.1, ...), custom_call_target="tpu_custom_call" | custom-call | flops 16106127360 | bytes 419430400 | tf_op jit(solution)/shard_map/pallas_call | solution.py:528
  113.4 5.3 %shard_map.171 = (f32[512,1024]{1,0:T(8,128)}, f32[512,1024]{1,0:T(8,128)}, f32[128,1024]{1,0:T(8,128)}, f32[128,1024]{1,0:T(8,128)}, f32[128,1024]{1,0:T(8,128)...) custom-call(bf16[2,2048,1024]{2,1,0:T(8,128)(2,1)S(1)} %get-tuple-element.11.fresh, ...), custom_call_target="tpu_custom_call" | custom-call | bytes 14680064 | tf_op jit(solution)/shard_map/pallas_call | solution.py:604

commit v3 on v2

--- a/solution.py
+++ b/solution.py
@@ -24,7 +24,7 @@
     "stage": (0.0, 0.33, 0.08, 0.0),
     "reduce": (0.5, 0.42, 0.17, 0.33),
     "directions": (0.5, 0.42, 0.17, 0.33),
-    "gather_z": (0.67, 0.5, 0.33, 0.33),
+    "gather_z": (0.58, 0.5, 0.33, 0.33),
     "gather": (0.83, 0.67, 0.67, 0.67),
     "end": (1.0, 1.0, 1.0, 1.0),
 }
@@ -59,6 +59,8 @@
     own,
     mid,
     recv_fs,
+    recv_end,
+    joint,
     low,
     dirs,
     mast,
@@ -81,6 +83,8 @@
     rp_r,
     rf_s,
     rf_r,
+    re_s,
+    re_r,
     dz_s,
     dz_r,
     dp_s,
@@ -207,45 +211,37 @@
         start, count = mrange(ff, ch, other)
         return mast.at[ch % 2, pl.ds(pl.multiple_of(start, count), count), :]
 
-    def my_turn(ch):
-        return (ry if ch % 2 == 0 else rx) == ch // 2
-
-    def swap():
-        for d, (source, exists, _, there) in enumerate(line):
-            for ch in range(CHUNKS):
-                piece = mpiece(source(1), ch)
-                mine_first = exists(1) & jnp.logical_not(there) & my_turn(ch)
-                arrived(piece, mz_s.at[d, 0, ch], mz_r.at[d, 0, ch], when=mine_first)
-                send(
-                    piece, mz_s.at[d, 1, ch], mz_r.at[d, 0, ch], (f, across[1 - ch % 2], t),
-                    when=mine_first,
-                )
+    def own_chunks(late, chunks=range(CHUNKS)):
+        for ch in chunks:
+            for d, (_, _, onto, there) in enumerate(line):
+                to_end = f == (nf - 2 if d == 0 else 1)
+                when = there
+                if late:
+                    when = there & to_end
+                elif ch >= CHUNKS // 2:
+                    when = there & jnp.logical_not(to_end)
+                if ch >= CHUNKS // 2 or not late:
+                    send(mpiece(f, ch), mz_s.at[d, 0, ch], mz_r.at[d, 0, ch], (onto, r, t), when=when)
 
     for p in range(2):
         load_m[p].wait()
         mast[p, block(f), :] = upd[p].astype(BF16)
-    for ch in range(CHUNKS):
-        for d, (_, _, onto, there) in enumerate(line):
-            to_end = f == (nf - 2 if d == 0 else 1)
-            send(
-                mpiece(f, ch), mz_s.at[d, 0, ch], mz_r.at[d, 0, ch], (onto, r, t),
-                when=there & (jnp.logical_not(to_end) | my_turn(ch)),
-            )
+    own_chunks(late=False)
 
     relays = [(j, ch) for j in range(1, nf) for ch in range(CHUNKS)]
+    late = [(1, ch) for ch in range(CHUNKS // 2, CHUNKS)]
+    final = relays[-(CHUNKS // 2):]
+    relays_last = [n for n in relays if n not in late and n not in final]
+    relays_last.insert(len(relays_last) - CHUNKS // 2, late[0])
+    relays_last += late[1:] + final
     done = [0, 0, 0, 0]
     last = jnp.logical_or(f == 0, f == nf - 1)
     inner = jnp.logical_not(last)
 
-    def land(j, ch, when, swapped=False):
-        for d, (source, exists, _, there) in enumerate(line):
-            due = exists(j) & when
-            if j == 1:
-                due = due & (jnp.logical_not(there | my_turn(ch)) if swapped else there)
-            elif swapped:
-                continue
+    def land(j, ch, when):
+        for d, (source, exists, _, _) in enumerate(line):
             piece = mpiece(source(j), ch)
-            arrived(piece, mz_s.at[d, j - 1, ch], mz_r.at[d, j - 1, ch], when=due)
+            arrived(piece, mz_s.at[d, j - 1, ch], mz_r.at[d, j - 1, ch], when=exists(j) & when)
 
     def onward(j, ch, ending):
         if j == nf - 1:
@@ -270,9 +266,8 @@
     def relay(point):
         ends = [max(d, round(share * len(relays))) for d, share in zip(done, SHARES[point])]
         for n in range(done[0], ends[0]):
-            land(*relays[n], last)
-            land(*relays[n], last, swapped=True)
-            aside(*relays[n], last)
+            land(*relays_last[n], last)
+            aside(*relays_last[n], last)
         landed = max(done[1:])
         for n in range(min(done[1:]), max(ends[1:])):
             if n >= landed:
@@ -334,9 +329,11 @@
     upper = rank // 2
     spans = (slice(0, upper), slice(upper, rank))
 
-    def product(p, rr):
-        at = pl.ds(pl.multiple_of(rr * width, width), width)
-        return jnp.dot(proj[p], c[p, :, at], preferred_element_type=F32)
+    def product(p, yy):
+        at = pl.ds(pl.multiple_of(yy * side * width, side * width), side * width)
+        both = jnp.dot(proj[p], c[p, :, at], preferred_element_type=F32)
+        left, right = both[:, :width], both[:, width:]
+        return jnp.where(rx == 0, left, right), jnp.where(rx == 0, right, left)
 
     def pass_part(s, m, a):
         send(part.at[s, m], rp_s.at[s, m], rp_r.at[s, m], (f, across[a], t), dst=recv.at[s, m])
@@ -350,16 +347,17 @@
             for i in range(TOKEN_TILES):
                 span = pl.ds(i * tile, tile)
                 arrived(proj.at[1 - t, :, span], pj_s.at[i], pj_r.at[i])
-        far = product(p, corner)
+        near_y, far = product(p, 1 - ry)
         for a in range(2):
             part[s, a] = far[spans[a]].astype(BF16)
             pass_part(s, a, a)
-        for a in range(2):
-            near = product(p, across[a])
-            part[s, 2 + a] = near[spans[a]].astype(BF16)
-            pass_part(s, 2 + a, a)
-            keep[s, 1 - a] = near[spans[1 - a]]
-        own[s] = product(p, r)
+        part[s, 3] = near_y[spans[1]].astype(BF16)
+        pass_part(s, 3, 1)
+        keep[s, 0] = near_y[spans[0]]
+        own[s], near_x = product(p, ry)
+        part[s, 2] = near_x[spans[0]].astype(BF16)
+        pass_part(s, 2, 0)
+        keep[s, 1] = near_x[spans[1]]
     relay("products")
 
     def rank_rows(ff):
@@ -370,7 +368,6 @@
             got_part(s, a)
             part[s, 4 + a] = (keep[s, a] + recv[s, a].astype(F32)).astype(BF16)
             pass_part(s, 4 + a, 1 - a)
-    swap()
     relay("stage")
     for s in range(2):
         for a in range(2):
@@ -380,11 +377,20 @@
             own[s, spans[a], :] = total
             mid[s, spans[a], :] = total.astype(BF16)
         for k in range(1, nf):
+            onto = fpeer(k)
+            piece = mid.at[s, rank_rows(onto), :]
+            to_last = (onto == 0) | (onto == nf - 1)
+            door = jnp.where(onto == 0, 1, nf - 2)
             send(
-                mid.at[s, rank_rows(fpeer(k)), :], rf_s.at[s, k - 1], rf_r.at[s, k - 1], (fpeer(k), r, t),
-                dst=recv_fs.at[s, k - 1],
+                piece, rf_s.at[s, k - 1], rf_r.at[s, k - 1], (onto, r, t), dst=recv_fs.at[s, k - 1],
+                when=jnp.logical_not(to_last),
+            )
+            send(
+                piece, re_s.at[s, k - 1], re_r.at[s, k - 1], (door, r, t), dst=recv_end.at[s, k - 1],
+                when=to_last & (f != door),
             )
     relay("reduce")
+    own_chunks(late=True, chunks=range(CHUNKS - 1))
 
     def dpiece(p, ff, rr, start=0, count=low_rows):
         at = pl.ds(pl.multiple_of(rr * width, width), width)
@@ -392,12 +398,27 @@
         return dirs.at[p, ranks, at]
 
     for s, p in enumerate(order):
+        for door, end, slots, slot in ((1, 0, range(nf - 2), nf - 2), (nf - 2, nf - 1, range(1, nf - 1), 0)):
+            @pl.when(f == door)
+            def _():
+                ranks = slice(end * low_rows, (end + 1) * low_rows)
+                total = own[s, ranks, :]
+                for i in slots:
+                    arrived(recv_end.at[s, i], re_s.at[s, i], re_r.at[s, i])
+                    total = total + recv_end[s, i].astype(F32)
+                joint[s] = total.astype(BF16)
+
+            send(
+                joint.at[s], rf_s.at[s, slot], rf_r.at[s, slot], (end, r, t), dst=recv_fs.at[s, slot],
+                when=f == door,
+            )
         for k in range(1, nf):
-            arrived(recv_fs.at[s, k - 1], rf_s.at[s, k - 1], rf_r.at[s, k - 1])
-        total = own[s, rank_rows(f), :]
-        for k in range(1, nf):
-            total = total + recv_fs[s, k - 1].astype(F32)
-        rounded = total.astype(BF16)
+            @pl.when(inner | ((f == 0) & (k == nf - 1)) | ((f == nf - 1) & (k == 1)))
+            def _():
+                arrived(recv_fs.at[s, k - 1], rf_s.at[s, k - 1], rf_r.at[s, k - 1])
+                own[s, rank_rows(f), :] = own[s, rank_rows(f), :] + recv_fs[s, k - 1].astype(F32)
+
+        rounded = own[s, rank_rows(f), :].astype(BF16)
         low[p, :, lane] = rounded
         again = rounded.astype(F32)
         new_first = beta_first * moments[p, :, lane] + (1.0 - beta_first) * again
@@ -422,6 +443,7 @@
             for a in range(2):
                 send(dpiece(p, src, r), dp_s.at[s, a, k], dp_r.at[s, a, k], (f, across[a], t))
     relay("gather_z")
+    own_chunks(late=True, chunks=range(CHUNKS - 1, CHUNKS))
     for k in range(1, nf):
         arrived(sums_z.at[k - 1], sz_s.at[k - 1], sz_r.at[k - 1])
     total = sums[...]
@@ -456,7 +478,6 @@
             src = fpeer(nf - k) if k else f
             for a in range(2):
                 arrived(dpiece(p, src, corner, a * low_half, low_half), dd_s.at[s, a, k], dd_r.at[s, a, k])
-    relay("end")
     arrived(sums_t.at[1], st_s, st_r)
     total = sums_t[0] + sums_t[1]
     scales = [1.0 / jnp.sqrt(jnp.sum(total[p]) / entries + scale_floor) for p in range(2)]
@@ -482,6 +503,35 @@
             span = pl.ds(i * unit, unit)
             fresh[p, at, :] = (mast[p, at, :].astype(F32) - step_rate * update).astype(BF16)
             upd[p, span, :] = update
+    relay("end")
+    def beside(j, ch, d):
+        source, exists, _, _ = line[d]
+        piece = mpiece(source(j), ch, other=True)
+        arrived(piece, mp_s.at[d, j - 1, ch], mp_r.at[d, j - 1, ch])
+
+    outer = [n for n in relays_last if n[0] in (1, nf - 1)]
+    early = outer[:-CHUNKS + 1]
+
+    def renew_outer(chunks, other):
+        for j, ch in chunks:
+            for d, (source, exists, _, _) in enumerate(line):
+                @pl.when(exists(j) & last)
+                def _():
+                    if other:
+                        beside(j, ch, d)
+                    start, count = mrange(source(j), ch, other)
+                    renew(ch % 2, start, count)
+
+    renew_outer(early, False)
+    @pl.loop(1, nf - 1)
+    def _(j):
+        for d, (source, exists, _, _) in enumerate(line):
+            @pl.when(exists(j) & (inner | (j > 1)))
+            def _():
+                for ch in range(CHUNKS):
+                    beside(j, ch, d)
+                renew_block(source(j))
+
     for j in range(1, nr):
         rsrc = rpeer(nr - j)
         at = pl.ds(pl.multiple_of(rsrc * width, width), width)
@@ -491,28 +541,9 @@
         moments[p] = beta_first * moments[p] + (1.0 - beta_first) * again
         moments[2 + p] = beta_second * moments[2 + p] + (1.0 - beta_second) * again * again
 
-    def beside(j, ch, d):
-        source, exists, _, _ = line[d]
-        piece = mpiece(source(j), ch, other=True)
-        arrived(piece, mp_s.at[d, j - 1, ch], mp_r.at[d, j - 1, ch], when=exists(j))
-
-    @pl.loop(1, nf - 1)
-    def _(j):
-        for d, (source, exists, _, _) in enumerate(line):
-            for ch in range(CHUNKS):
-                beside(j, ch, d)
-            guarded(lambda: renew_block(source(j)), exists(j))
-
-    j = nf - 1
-    for ch in range(CHUNKS):
-        for d, (source, exists, _, _) in enumerate(line):
-            start, count = mrange(source(j), ch)
-            guarded(lambda: renew(ch % 2, start, count), exists(j))
-    for ch in range(CHUNKS):
-        for d, (source, exists, _, _) in enumerate(line):
-            beside(j, ch, d)
-            start, count = mrange(source(j), ch, other=True)
-            guarded(lambda: renew(ch % 2, start, count), exists(j))
+    renew_outer(early, True)
+    renew_outer(outer[-CHUNKS + 1:], False)
+    renew_outer(outer[-CHUNKS + 1:], True)
     for copy, when in started:
         guarded(copy.wait_send, when)
 
@@ -546,6 +577,8 @@
             pltpu.VMEM((2, rank, width), F32),
             pltpu.VMEM((2, rank, width), BF16),
             pltpu.VMEM((2, nf - 1, low_rows, width), BF16),
+            pltpu.VMEM((2, nf - 1, low_rows, width), BF16),
+            pltpu.VMEM((2, low_rows, width), BF16),
             pltpu.VMEM((2, low_rows, cols), BF16),
             pltpu.VMEM((2, rank, cols), BF16),
             pltpu.VMEM((2, model, cols), BF16),
@@ -561,6 +594,7 @@
             dma,
             *pair(TOKEN_TILES),
             *pair(2, 6),
+            *pair(2, nf - 1),
             *pair(2, nf - 1),
             *pair(2, nf - 1),
             *pair(2, 2, nf),

time: 119 us -> 117 us (0.983)
  Pallas kernels: 118 us -> 116 us
    pallas_call x1, Pallas kernels: 113 us -> 110 us  [gather_all(): pl.pallas_call(functools.partial(kernel, nf, nr, entries), out_shape=(plt...]
where the time goes in v3:
time: 117 us; the launch traced here: 116 us
  Pallas kernels  116 us (99%)
    pallas_call x1, Pallas kernels, gather_all(): pl.pallas_call(functools.partial(kernel, nf, nr, entries), out_shape=(plt...  110 us
    pallas_call x1, Pallas kernels, finish(): pl.pallas_call(finish_kernel, out_shape=(*[shape(upd.shape[1:], F32)] * 2...  5.31 us

profile of v3, /device:TPU:0, one launch (start us, length us, event | category | flops | bytes accessed | tf_op | source)
XLA Modules:
  0.0 116.4 jit_solution(11313747154190828666)
XLA Ops:
  0.6 110.2 %shard_map.170 = (bf16[2,2048,1024]{2,1,0:T(8,128)(2,1)S(1)}, f32[2,512,1024]{2,1,0:T(8,128)S(1)}, f32[4,128,1024]{2,1,0:T(8,128)S(1)}) custom-call(bf16[1536,2048]{1,0:T(8,128)(2,1)} %x_hbm.1, bf16[1536,1024]{1,0:T(8,128)(2,1)} %c0_hbm.1, bf16[1536,1024]{1,0:T(8,128)(2,1)} %c1_hbm.1, bf16[512,512]{1,0:T(8,128)(2,1)} %fac0_hbm.1, bf16[512,512]{1,0:T(8,128)(2,1)} %fac1_hbm.1, ...), custom_call_target="tpu_custom_call" | custom-call | flops 16106127360 | bytes 419430400 | tf_op jit(solution)/shard_map/pallas_call | solution.py:559
  110.9 5.3 %shard_map.171 = (f32[512,1024]{1,0:T(8,128)}, f32[512,1024]{1,0:T(8,128)}, f32[128,1024]{1,0:T(8,128)}, f32[128,1024]{1,0:T(8,128)}, f32[128,1024]{1,0:T(8,128)...) custom-call(bf16[2,2048,1024]{2,1,0:T(8,128)(2,1)S(1)} %get-tuple-element.11.fresh, ...), custom_call_target="tpu_custom_call" | custom-call | bytes 14680064 | tf_op jit(solution)/shard_map/pallas_call | solution.py:638

commit v4 on v3

--- a/solution.py
+++ b/solution.py
@@ -23,7 +23,7 @@
     "products": (0.0, 0.25, 0.08, 0.0),
     "stage": (0.0, 0.33, 0.08, 0.0),
     "reduce": (0.5, 0.42, 0.17, 0.33),
-    "directions": (0.5, 0.42, 0.17, 0.33),
+    "directions": (0.58, 0.42, 0.25, 0.33),
     "gather_z": (0.58, 0.5, 0.33, 0.33),
     "gather": (0.83, 0.67, 0.67, 0.67),
     "end": (1.0, 1.0, 1.0, 1.0),

time: 117 us -> 117 us (level)
  no operation moved by 1% of the time
where the time goes in v4:
time: 117 us; the launch traced here: 116 us
  Pallas kernels  116 us (99%)
    pallas_call x1, Pallas kernels, gather_all(): pl.pallas_call(functools.partial(kernel, nf, nr, entries), out_shape=(plt...  110 us
    pallas_call x1, Pallas kernels, finish(): pl.pallas_call(finish_kernel, out_shape=(*[shape(upd.shape[1:], F32)] * 2...  5.31 us

profile of v4, /device:TPU:0, one launch (start us, length us, event | category | flops | bytes accessed | tf_op | source)
XLA Modules:
  0.0 116.4 jit_solution(3042885302604369337)
XLA Ops:
  0.6 110.2 %shard_map.170 = (bf16[2,2048,1024]{2,1,0:T(8,128)(2,1)S(1)}, f32[2,512,1024]{2,1,0:T(8,128)S(1)}, f32[4,128,1024]{2,1,0:T(8,128)S(1)}) custom-call(bf16[1536,2048]{1,0:T(8,128)(2,1)} %x_hbm.1, bf16[1536,1024]{1,0:T(8,128)(2,1)} %c0_hbm.1, bf16[1536,1024]{1,0:T(8,128)(2,1)} %c1_hbm.1, bf16[512,512]{1,0:T(8,128)(2,1)} %fac0_hbm.1, bf16[512,512]{1,0:T(8,128)(2,1)} %fac1_hbm.1, ...), custom_call_target="tpu_custom_call" | custom-call | flops 16106127360 | bytes 419430400 | tf_op jit(solution)/shard_map/pallas_call | solution.py:559
  110.9 5.3 %shard_map.171 = (f32[512,1024]{1,0:T(8,128)}, f32[512,1024]{1,0:T(8,128)}, f32[128,1024]{1,0:T(8,128)}, f32[128,1024]{1,0:T(8,128)}, f32[128,1024]{1,0:T(8,128)...) custom-call(bf16[2,2048,1024]{2,1,0:T(8,128)(2,1)S(1)} %get-tuple-element.11.fresh, ...), custom_call_target="tpu_custom_call" | custom-call | bytes 14680064 | tf_op jit(solution)/shard_map/pallas_call | solution.py:638
